TPU v7x, 32 devices: a whole 2x2x4 slice. The times are simulated.
32 devices in a mesh: sp: 8 (over z, y), tp: 4 (over x, core).
Axes of the slice: x: 2, y: 2, z: 4, core: 2. Of those that a mesh axis runs over, the one named last changes fastest.
Arguments:
- hidden: bfloat16 [2048, 2048], P('sp'), may hold values from -6 to 6
- cotangent: bfloat16 [2048, 2048], P('sp'), may hold values from -6 to 6
- retained: bfloat16 [2048, 2048], P('sp', 'tp'), may hold values from -6 to 6
- queries: bfloat16 [2048, 1024], P('sp', 'tp'), may hold values from -1.5 to 1.5
- key_rows: bfloat16 [2048, 1024], P('sp', 'tp'), may hold values from -1.5 to 1.5
- value_rows: bfloat16 [2048, 2048], P('sp', 'tp'), may hold values from -0.25 to 0.25
- routes: int32 [2048, 2], P('sp'), may hold values from 0 to 7, all different within a row; in each aligned block of 256 rows (0 to 255, 256 to 511, ...) at most 96 rows name the same one
- route_weight: float32 [2048, 2], P('sp'), may hold values from 0.2 to 1.5
- gate_weight: bfloat16 [8, 2048, 1024], P('sp', None, 'tp'), may hold values from -0.125 to 0.125
- up_weight: bfloat16 [8, 2048, 1024], P('sp', None, 'tp'), may hold values from -0.125 to 0.125
- down_weight: bfloat16 [8, 1024, 2048], P('sp', 'tp'), may hold values from -0.1875 to 0.1875
- out_weight: bfloat16 [2048, 2048], P(None, 'tp'), may hold values from -0.125 to 0.125
Outputs:
- gate_grad: float32 [8, 2048, 1024], P('sp', None, 'tp')
- up_grad: float32 [8, 2048, 1024], P('sp', None, 'tp')
- down_grad: float32 [8, 1024, 2048], P('sp', 'tp')
- proj_grad: float32 [2048, 2048], P('sp', 'tp')
- query_gradient: float32 [2048, 1024], P('sp', 'tp')
- key_gradient: float32 [2048, 1024], P('sp', 'tp')
- value_gradient: float32 [2048, 2048], P('sp', 'tp')
Inputs may be any that keep to these rules, and one draw needn't show every extreme that they name: `routes`: each row names 2 different experts; among the 256 rows of one index of sp no expert is named more than 96 times, a bound that some block reaches.
All inputs are finite; a program needn't handle non-finite values.
Results may differ from a plain program's by a relative error of at most 0.013.
Values may be sent and summed in bfloat16 or wider, within the bound.
A program may use at most 128 MiB of HBM per device.

v0:
```python
import math

import jax
import jax.numpy as jnp
from jax import lax
from jax.sharding import PartitionSpec as P

H = 4
DK = 256
DV = 512


def carried(part, log_span, axis, reverse):
    count = lax.axis_size(axis)
    held = part
    ahead = jnp.zeros_like(part)
    step = 1
    while step < count:
        pairs = [(i + step, i) if reverse else (i, i + step) for i in range(count - step)]
        got = lax.ppermute(held.astype(jnp.bfloat16), axis, pairs).astype(jnp.float32)
        ahead = ahead + jnp.exp(log_span * (step - 1.0))[:, None, None] * got
        held = held + jnp.exp(log_span * float(step))[:, None, None] * got
        step *= 2
    return ahead


def scattered_sum(part, axis):
    count = lax.axis_size(axis)
    me = lax.axis_index(axis)
    if count & (count - 1):
        return lax.psum_scatter(part, axis, scatter_dimension=2, tiled=True)
    wide = part.shape[2] // count
    pieces = {
        k: lax.dynamic_slice_in_dim(part, jnp.bitwise_xor(me, k) * wide, wide, 2)
        for k in range(count)
    }
    bit = 1
    while bit < count:
        pairs = [(i, i ^ bit) for i in range(count)]
        for k in sorted(k for k in pieces if k & bit):
            got = lax.ppermute(pieces.pop(k), axis, pairs)
            kept = pieces[k ^ bit].astype(jnp.float32)
            pieces[k ^ bit] = (kept + got.astype(jnp.float32)).astype(jnp.bfloat16)
        bit *= 2
    return pieces[0]


def expert_backward(inputs, upstream, gate_matrix, up_matrix, down_matrix):
    along_rows = (((0,), (0,)), ((), ()))
    along_cols = (((1,), (1,)), ((), ()))
    gate_pre = jnp.dot(inputs, gate_matrix, preferred_element_type=jnp.float32)
    up_pre = jnp.dot(inputs, up_matrix, preferred_element_type=jnp.float32)
    sigma = jax.nn.sigmoid(gate_pre)
    active = gate_pre * sigma
    product = (active * up_pre).astype(jnp.bfloat16)
    down_part = lax.dot_general(product, upstream, along_rows, preferred_element_type=jnp.float32)
    unit_grad = lax.dot_general(
        upstream, down_matrix, along_cols, preferred_element_type=jnp.float32
    )
    gate_term = (unit_grad * up_pre * sigma * (1.0 + gate_pre * (1.0 - sigma))).astype(jnp.bfloat16)
    up_term = (unit_grad * active).astype(jnp.bfloat16)
    gate_part = lax.dot_general(inputs, gate_term, along_rows, preferred_element_type=jnp.float32)
    up_part = lax.dot_general(inputs, up_term, along_rows, preferred_element_type=jnp.float32)
    row_part = lax.dot_general(
        gate_term, gate_matrix, along_cols, preferred_element_type=jnp.float32
    )
    row_part = row_part + lax.dot_general(
        up_term, up_matrix, along_cols, preferred_element_type=jnp.float32
    )
    return (gate_part, up_part, down_part, row_part.astype(jnp.bfloat16))


def head_rates(head_ids, total_tokens):
    ids = head_ids.astype(jnp.float32)
    exponent = jnp.where(2 * head_ids < H, -5.0 - ids, -math.log2(total_tokens) - (ids - H // 2))
    log_gamma = jnp.log1p(-jnp.exp2(exponent))
    scale = jnp.sqrt(-jnp.expm1(2.0 * log_gamma))
    return (log_gamma, scale)


def local(
    hidden,
    cotangent,
    retained,
    queries,
    key_rows,
    value_rows,
    routes,
    route_weight,
    gate_weight,
    up_weight,
    down_weight,
    out_weight,
):
    sp_count = lax.axis_size("sp")
    tp_count = lax.axis_size("tp")
    tok_local = hidden.shape[0]
    width = hidden.shape[1]
    top_count = routes.shape[1]
    experts_all = gate_weight.shape[0] * sp_count
    capacity = 3 * tok_local * top_count // (2 * experts_all)
    ids = jnp.arange(experts_all, dtype=jnp.int32)[:, None]
    named = [routes[:, r][None, :] == ids for r in range(top_count)]
    member = sum(m.astype(jnp.float32) for m in named)
    slot_weight = sum(jnp.where(m, route_weight[:, r][None, :], 0.0) for r, m in enumerate(named))
    order = jnp.arange(tok_local, dtype=jnp.int32)
    earlier = (order[:, None] < order[None, :]).astype(jnp.bfloat16)
    rank = jnp.dot(member.astype(jnp.bfloat16), earlier, preferred_element_type=jnp.float32)
    rank = jnp.where(member > 0.0, rank, -1.0).astype(jnp.int32)
    hit = rank[:, None, :] == jnp.arange(capacity, dtype=jnp.int32)[None, :, None]
    place_rows = hit.astype(jnp.bfloat16).reshape(experts_all * capacity, tok_local)
    row_weight = jnp.sum(jnp.where(hit, slot_weight[:, None, :], 0.0), axis=2).reshape(-1, 1)
    col_width = width // tp_count
    col_start = lax.axis_index("tp") * col_width
    hid_cols = lax.dynamic_slice_in_dim(hidden, col_start, col_width, 1)
    cot_cols = lax.dynamic_slice_in_dim(cotangent, col_start, col_width, 1)

    def to_experts(rows):
        rows = rows.astype(jnp.bfloat16).reshape(experts_all, capacity, col_width)
        return lax.all_to_all(rows, "sp", split_axis=0, concat_axis=1, tiled=True)

    in_cols = to_experts(jnp.dot(place_rows, hid_cols, preferred_element_type=jnp.float32))
    in_cols, cot_cols = lax.optimization_barrier((in_cols, cot_cols))
    up_cols = to_experts(
        row_weight * jnp.dot(place_rows, cot_cols, preferred_element_type=jnp.float32)
    )
    heads_local = queries.shape[1] // DK
    head_ids = lax.axis_index("tp") * heads_local + jnp.arange(heads_local, dtype=jnp.int32)
    log_gamma, scale = head_rates(head_ids, tok_local * sp_count)
    key_rows, value_rows, up_cols = lax.optimization_barrier((key_rows, value_rows, up_cols))
    query_three = queries.reshape(tok_local, heads_local, DK)
    key_three = key_rows.reshape(tok_local, heads_local, DK)
    value_three = value_rows.reshape(tok_local, heads_local, DV)
    place = jnp.arange(tok_local, dtype=jnp.float32)
    suffix_decay = jnp.exp(log_gamma[None, :] * (tok_local - place[:, None]))
    prefix_decay = jnp.exp(log_gamma[None, :] * (place[:, None] + 1.0))
    forward_shard_local = jnp.einsum(
        "ibz,ibm->bzm",
        (key_three * suffix_decay[:, :, None]).astype(jnp.bfloat16),
        value_three,
        preferred_element_type=jnp.float32,
    )
    log_span = log_gamma * tok_local
    prior_positions = carried(forward_shard_local, log_span, "sp", False).astype(jnp.bfloat16)
    got_in = lax.all_gather(in_cols, "tp", axis=2, tiled=True)
    got_up = lax.all_gather(up_cols, "tp", axis=2, tiled=True)
    retained, got_up = lax.optimization_barrier((retained, got_up))
    retained_all = lax.all_gather(retained, "sp", axis=0, tiled=True)
    gate_grad, up_grad, down_grad, row_part = jax.vmap(expert_backward)(
        got_in, got_up, gate_weight, up_weight, down_weight
    )
    row_part, prior_positions = lax.optimization_barrier((row_part, prior_positions))
    row_grad = scattered_sum(row_part, "tp")
    row_grad = row_grad.reshape(-1, sp_count, capacity, col_width).swapaxes(0, 1)
    returned = lax.all_to_all(row_grad, "sp", split_axis=0, concat_axis=0, tiled=True)
    returned, retained_all = lax.optimization_barrier((returned, retained_all))
    routed = lax.dot_general(
        place_rows,
        returned.reshape(-1, col_width),
        (((0,), (0,)), ((), ())),
        preferred_element_type=jnp.float32,
    )
    layer_cols = (cot_cols.astype(jnp.float32) + routed).astype(jnp.bfloat16)
    layer_grad = lax.all_gather(layer_cols, "tp", axis=1, tiled=True)
    mixed_grad = jnp.dot(layer_grad, out_weight, preferred_element_type=jnp.float32).astype(
        jnp.bfloat16
    )
    share = tok_local // tp_count
    share_rows = lax.dynamic_slice_in_dim(layer_grad, lax.axis_index("tp") * share, share, 0)
    share_rows = share_rows.reshape(share, sp_count, -1).swapaxes(0, 1)
    block_rows = lax.all_to_all(share_rows, "sp", split_axis=0, concat_axis=0, tiled=True)
    block_all = lax.all_gather(block_rows, "tp", axis=1, tiled=True)
    proj_grad = lax.dot_general(
        block_all.reshape(sp_count * tok_local, -1),
        retained_all,
        (((0,), (0,)), ((), ())),
        preferred_element_type=jnp.float32,
    )
    output_grad_three = mixed_grad.reshape(tok_local, heads_local, DV)
    backward_local = jnp.einsum(
        "stz,stb->tzb",
        (query_three * prefix_decay[:, :, None]).astype(jnp.bfloat16),
        output_grad_three,
        preferred_element_type=jnp.float32,
    )
    later_positions = carried(backward_local, log_span, "sp", True).astype(jnp.bfloat16)
    gap = place[:, None] - place[None, :]
    weight = jnp.where(
        gap[None] >= 0,
        scale[:, None, None] * jnp.exp(log_gamma[:, None, None] * jnp.maximum(gap, 0.0)[None]),
        0.0,
    )
    local_value_grad = (
        jnp.einsum(
            "ihv,jhv->hij", output_grad_three, value_three, preferred_element_type=jnp.float32
        )
        * weight
    ).astype(jnp.bfloat16)
    local_query_key = (
        jnp.einsum("ihd,jhd->hij", query_three, key_three, preferred_element_type=jnp.float32)
        * weight
    ).astype(jnp.bfloat16)
    leading_span = (scale[None, :] * jnp.exp(log_gamma[None, :] * place[:, None]))[:, :, None]
    trailing_span = (
        scale[None, :] * jnp.exp(log_gamma[None, :] * (tok_local - 1.0 - place[:, None]))
    )[:, :, None]
    query_gradient = jnp.einsum(
        "zby,yze->bze", local_value_grad, key_three, preferred_element_type=jnp.float32
    )
    query_gradient = query_gradient + leading_span * jnp.einsum(
        "eal,gel->gea", prior_positions, output_grad_three, preferred_element_type=jnp.float32
    )
    key_gradient = jnp.einsum(
        "lcx,clo->xlo", local_value_grad, query_three, preferred_element_type=jnp.float32
    )
    key_gradient = key_gradient + trailing_span * jnp.einsum(
        "gta,wga->wgt", later_positions, value_three, preferred_element_type=jnp.float32
    )
    value_gradient = jnp.einsum(
        "upb,puk->buk", local_query_key, output_grad_three, preferred_element_type=jnp.float32
    )
    value_gradient = value_gradient + trailing_span * jnp.einsum(
        "tdx,btd->btx", later_positions, key_three, preferred_element_type=jnp.float32
    )
    return (
        gate_grad,
        up_grad,
        down_grad,
        proj_grad,
        query_gradient.reshape(tok_local, heads_local * DK),
        key_gradient.reshape(tok_local, heads_local * DK),
        value_gradient.reshape(tok_local, heads_local * DV),
    )


def solution(mesh):
    return jax.shard_map(
        local,
        mesh=mesh,
        in_specs=(
            P("sp", None),
            P("sp", None),
            P("sp", "tp"),
            P("sp", "tp"),
            P("sp", "tp"),
            P("sp", "tp"),
            P("sp", None),
            P("sp", None),
            P("sp", None, "tp"),
            P("sp", None, "tp"),
            P("sp", "tp", None),
            P(None, "tp"),
        ),
        out_specs=(
            P("sp", None, "tp"),
            P("sp", None, "tp"),
            P("sp", "tp", None),
            P("sp", "tp"),
            P("sp", "tp"),
            P("sp", "tp"),
            P("sp", "tp"),
        ),
        check_vma=False,
    )
```

profile of v0, /device:TPU:0, one launch (start us, length us, event | category | flops | bytes accessed | tf_op | source)
XLA Modules:
  0.0 260.2 jit_solution(12904487901622721336)
XLA Ops:
  10.7 7.4 %all-to-all-start = ((bf16[8,96,512]{2,1,0:T(8,128)(2,1)}), bf16[8,96,512]{2,1,0:T(8,128)(2,1)S(1)}, u32[]{:S(2)}, u32[]{:S(2)}) async-start(bf16[8,96,512]{2,1,0:T(8,128)(2,1)} %bitcast.164), calls=%async_computation | async-start | bytes 1572864 | tf_op jit(solution)/shard_map/all_to_all | solution.py:120
  19.1 19.1 %all-to-all-done = bf16[8,96,512]{2,1,0:T(8,128)(2,1)S(1)} async-done(((bf16[8,96,512]{2,1,0:T(8,128)(2,1)}), bf16[8,96,512]{2,1,0:T(8,128)(2,1)S(1)}, u32[]{:S(2)}, u32[]{:S(2)}) %all-to-all-start) | async-done | bytes 786464 | tf_op jit(solution)/shard_map/all_to_all | solution.py:120
  40.0 23.8 %all_to_all.34 = bf16[8,96,512]{2,1,0:T(8,128)(2,1)} all-to-all(bf16[8,96,512]{2,1,0:T(8,128)(2,1)S(1)} %bitcast.165), channel_id=1, replica_groups=mesh['sp'=8,'tp'=4] {'sp'}, dimensions={0} | all-to-all | bytes 1572864 | tf_op jit(solution)/shard_map/all_to_all | solution.py:120
  64.3 3.4 %collective-permute-start = (bf16[1,256,512]{2,1,0:T(8,128)(2,1)S(1)}, bf16[1,256,512]{2,1,0:T(8,128)(2,1)S(1)}, u32[]{:S(2)}, u32[]{:S(2)}) collective-permute-start(bf16[1,256,512]{2,1,0:T(8,128)(2,1)S(1)} %convert_bitcast_fusion.1), channel_id=1, source_target_pairs={{0,4},{4,8},{8,12},{12,16},{16,20},{20,24},{24,28},{1,5},{5,9},{9,... | collective-permute-start | bytes 786440 | tf_op jit(solution)/shard_map/ppermute | solution.py:20
  67.7 4.5 %collective-permute-done = bf16[1,256,512]{2,1,0:T(8,128)(2,1)S(1)} collective-permute-done((bf16[1,256,512]{2,1,0:T(8,128)(2,1)S(1)}, bf16[1,256,512]{2,1,0:T(8,128)(2,1)S(1)}, u32[]{:S(2)}, u32[]{:S(2)}) %collective-permute-start) | collective-permute-done | bytes 262176 | tf_op jit(solution)/shard_map/ppermute | solution.py:20
  73.0 4.6 %collective-permute-start.1 = (bf16[1,256,512]{2,1,0:T(8,128)(2,1)}, bf16[1,256,512]{2,1,0:T(8,128)(2,1)S(1)}, u32[]{:S(2)}, u32[]{:S(2)}) collective-permute-start(bf16[1,256,512]{2,1,0:T(8,128)(2,1)} %fusion.56), channel_id=1, source_target_pairs={{0,8},{4,12},{8,16},{12,20},{16,24},{20,28},{1,9},{5,13},{9,17},{1... | collective-permute-start | bytes 786440 | tf_op jit(solution)/shard_map/ppermute | solution.py:20
  77.6 4.1 %collective-permute-done.1 = bf16[1,256,512]{2,1,0:T(8,128)(2,1)S(1)} collective-permute-done((bf16[1,256,512]{2,1,0:T(8,128)(2,1)}, bf16[1,256,512]{2,1,0:T(8,128)(2,1)S(1)}, u32[]{:S(2)}, u32[]{:S(2)}) %collective-permute-start.1) | collective-permute-done | bytes 262176 | tf_op jit(solution)/shard_map/ppermute | solution.py:20
  82.6 5.0 %collective-permute-start.2 = (bf16[1,256,512]{2,1,0:T(8,128)(2,1)}, bf16[1,256,512]{2,1,0:T(8,128)(2,1)S(1)}, u32[]{:S(2)}, u32[]{:S(2)}) collective-permute-start(bf16[1,256,512]{2,1,0:T(8,128)(2,1)} %fusion.48), channel_id=1, source_target_pairs={{0,16},{4,20},{8,24},{12,28},{1,17},{5,21},{9,25},{13,29},{2,18},{... | collective-permute-start | bytes 786440 | tf_op jit(solution)/shard_map/ppermute | solution.py:20
  87.7 4.1 %collective-permute-done.2 = bf16[1,256,512]{2,1,0:T(8,128)(2,1)S(1)} collective-permute-done((bf16[1,256,512]{2,1,0:T(8,128)(2,1)}, bf16[1,256,512]{2,1,0:T(8,128)(2,1)S(1)}, u32[]{:S(2)}, u32[]{:S(2)}) %collective-permute-start.2) | collective-permute-done | bytes 262176 | tf_op jit(solution)/shard_map/ppermute | solution.py:20
  92.7 4.2 %fusion.8 = f32[768,256]{1,0:T(8,128)} fusion(bf16[1,768,2048]{2,1,0:T(8,128)(2,1)} %all-gather.6.cloned.1.call-done, bf16[1,2048,256]{2,1,0:T(8,128)(2,1)} %param.20), kind=kOutput, calls=%fused_computation.9 | convolution fusion | flops 805306368 | bytes 4980736 | tf_op jit(solution)/shard_map/vmap()/dot_general | solution.py:51
  98.8 3.9 %multiply_convert_fusion.2 = (bf16[768,256]{1,0:T(8,128)(2,1)S(1)}, bf16[768,256]{1,0:T(8,128)(2,1)S(1)}) fusion(f32[768,256]{1,0:T(8,128)} %fusion.8, f32[768,256]{1,0:T(8,128)} %fusion.10, bf16[1,256,2048]{2,1,0:T(8,128)(2,1)} %param.22, bf16[1,768,2048]{2,1,0:T(8,128)(2,1)} %all-gather.8.cloned.1.call-done), kind=kOutput, calls=%fused_computation.55 | convolution fusion | flops 807862272 | bytes 6553600 | tf_op jit(solution)/shard_map/vmap()/dot_general | solution.py:57
  103.4 3.7 %fusion.36 = f32[768,2048]{1,0:T(8,128)} fusion(bf16[768,256]{1,0:T(8,128)(2,1)S(1)} %get-tuple-element.67, bf16[1,2048,256]{2,1,0:T(8,128)(2,1)S(1)} %copy-done.6), kind=kOutput, calls=%fused_computation.47 | convolution fusion | flops 805306368 | bytes 7733248 | tf_op jit(solution)/shard_map/vmap()/dot_general | solution.py:64
  107.2 4.1 %fusion.12 = bf16[1,768,2048]{2,1,0:T(8,128)(2,1)S(1)} fusion(f32[768,2048]{1,0:T(8,128)} %fusion.36, bf16[768,256]{1,0:T(8,128)(2,1)S(1)} %get-tuple-element.66, bf16[1,2048,256]{2,1,0:T(8,128)(2,1)} %param.21), kind=kOutput, calls=%fused_computation.13 | convolution fusion | flops 808452096 | bytes 10878976 | tf_op jit(solution)/shard_map/vmap()/dot_general | solution.py:67
  119.6 18.1 %collective-permute-done.5 = bf16[1,768,512]{2,1,0:T(8,128)(2,1)S(1)} collective-permute-done((bf16[1,768,512]{2,1,0:T(8,128)(2,1)S(1)}, bf16[1,768,512]{2,1,0:T(8,128)(2,1)S(1)}, u32[]{:S(2)}, u32[]{:S(2)}) %collective-permute-start.5) | collective-permute-done | bytes 786464 | tf_op jit(solution)/shard_map/ppermute | solution.py:41
  140.1 10.4 %all-to-all-start.2 = ((bf16[8,1,96,512]{3,2,1,0:T(8,128)(2,1)}), bf16[8,1,96,512]{3,2,1,0:T(8,128)(2,1)S(1)}, u32[]{:S(2)}, u32[]{:S(2)}) async-start(bf16[8,1,96,512]{3,2,1,0:T(8,128)(2,1)} %bitcast.166), calls=%async_computation.2 | async-start | bytes 1572864 | tf_op jit(solution)/shard_map/all_to_all | solution.py:155
  150.6 26.6 %all-to-all-done.2 = bf16[8,1,96,512]{3,2,1,0:T(8,128)(2,1)S(1)} async-done(((bf16[8,1,96,512]{3,2,1,0:T(8,128)(2,1)}), bf16[8,1,96,512]{3,2,1,0:T(8,128)(2,1)S(1)}, u32[]{:S(2)}, u32[]{:S(2)}) %all-to-all-start.2) | async-done | bytes 786464 | tf_op jit(solution)/shard_map/all_to_all | solution.py:155
  178.5 4.4 %fusion.13 = f32[1,2048,256]{2,1,0:T(8,128)} fusion(bf16[768,256]{1,0:T(8,128)(2,1)} %copy-done.5, bf16[1,768,2048]{2,1,0:T(8,128)(2,1)} %all-gather.6.cloned.1.call-done), kind=kOutput, calls=%fused_computation.14 | convolution fusion | flops 805306368 | bytes 5636096 | tf_op jit(solution)/shard_map/vmap()/dot_general | solution.py:62
  185.3 8.2 %all-gather.12.cloned.1.call-done = bf16[256,2048]{1,0:T(8,128)(2,1)} async-done(((bf16[256,512]{1,0:T(8,128)(2,1)}), bf16[256,2048]{1,0:T(8,128)(2,1)}) %all-gather.12.cloned.1.call-update) | async-done | bytes 1048592 | tf_op jit(solution)/shard_map/all_gather | solution.py:164
  195.4 5.5 %all-to-all-start.3 = ((bf16[8,64,256]{2,1,0:T(8,128)(2,1)}), bf16[8,64,256]{2,1,0:T(8,128)(2,1)}, u32[]{:S(2)}, u32[]{:S(2)}) async-start(bf16[8,64,256]{2,1,0:T(8,128)(2,1)} %copy.43), calls=%async_computation.3 | async-start | bytes 524288 | tf_op jit(solution)/shard_map/all_to_all | solution.py:171
  204.9 3.4 %fusion.16 = f32[1,2048,256]{2,1,0:T(8,128)} fusion(bf16[768,256]{1,0:T(8,128)(2,1)} %copy-done.9, bf16[1,768,2048]{2,1,0:T(8,128)(2,1)S(1)} %copy-done.12), kind=kOutput, calls=%fused_computation.15 | convolution fusion | flops 805306368 | bytes 5636096 | tf_op jit(solution)/shard_map/vmap()/dot_general | solution.py:63
  208.3 6.1 %collective-permute-done.6 = bf16[1,256,512]{2,1,0:T(8,128)(2,1)S(1)} collective-permute-done((bf16[1,256,512]{2,1,0:T(8,128)(2,1)S(1)}, bf16[1,256,512]{2,1,0:T(8,128)(2,1)S(1)}, u32[]{:S(2)}, u32[]{:S(2)}) %collective-permute-start.6) | collective-permute-done | bytes 262176 | tf_op jit(solution)/shard_map/ppermute | solution.py:20
  219.8 5.3 %collective-permute-done.7 = bf16[1,256,512]{2,1,0:T(8,128)(2,1)} collective-permute-done((bf16[1,256,512]{2,1,0:T(8,128)(2,1)}, bf16[1,256,512]{2,1,0:T(8,128)(2,1)}, u32[]{:S(2)}, u32[]{:S(2)}) %collective-permute-start.7) | collective-permute-done | bytes 262176 | tf_op jit(solution)/shard_map/ppermute | solution.py:20
  230.4 11.9 %collective-permute-done.8 = bf16[1,256,512]{2,1,0:T(8,128)(2,1)} collective-permute-done((bf16[1,256,512]{2,1,0:T(8,128)(2,1)}, bf16[1,256,512]{2,1,0:T(8,128)(2,1)}, u32[]{:S(2)}, u32[]{:S(2)}) %collective-permute-start.8) | collective-permute-done | bytes 262176 | tf_op jit(solution)/shard_map/ppermute | solution.py:20
  250.5 3.1 %fusion.80 = f32[256,512]{1,0:T(8,128)} fusion(bf16[2048,256]{1,0:T(8,128)(2,1)S(1)} %bitcast.168, bf16[2048,512]{1,0:T(8,128)(2,1)} %all-gather.10.cloned.1.call-done), kind=kOutput, calls=%fused_computation.122 | convolution fusion | flops 536870912 | bytes 3670016 | tf_op jit(solution)/shard_map/dot_general | solution.py:173
  (102 shorter events, 50.5 us)
Async XLA Ops:
  7.2 193.9 %copy-start = (bf16[2048,512]{1,0:T(8,128)(2,1)S(1)}, bf16[2048,512]{1,0:T(8,128)(2,1)}, u32[]{:S(2)}) copy-start(bf16[2048,512]{1,0:T(8,128)(2,1)} %param.23) | copy-start | bytes 6291460
  7.2 32.1 %copy-start.10 = (f32[256,2]{0,1:T(2,128)S(1)}, f32[256,2]{0,1:T(2,128)}, u32[]{:S(2)}) copy-start(f32[256,2]{0,1:T(2,128)} %param.19) | copy-start | bytes 6148
  10.7 53.2 %copy-start.3 = (bf16[256,256]{1,0:T(8,128)(2,1)S(1)}, bf16[256,256]{1,0:T(8,128)(2,1)}, u32[]{:S(2)}) copy-start(bf16[256,256]{1,0:T(8,128)(2,1)} %param.16) | copy-start | bytes 393220
  10.7 27.6 %all-to-all-start = ((bf16[8,96,512]{2,1,0:T(8,128)(2,1)}), bf16[8,96,512]{2,1,0:T(8,128)(2,1)S(1)}, u32[]{:S(2)}, u32[]{:S(2)}) async-start(bf16[8,96,512]{2,1,0:T(8,128)(2,1)} %bitcast.164), calls=%async_computation | async-start | bytes 1572864 | tf_op jit(solution)/shard_map/all_to_all | solution.py:120
  18.1 74.6 %all-gather.6.cloned.1.call-start = ((), (), s32[]{:S(2)}) async-start(), calls=%async_computation.4 | async-start | bytes 3932160 | tf_op jit(solution)/shard_map/all_gather | solution.py:145
  39.2 24.7 %copy-start.7 = (bf16[256,512]{1,0:T(8,128)(2,1)S(1)}, bf16[256,512]{1,0:T(8,128)(2,1)}, u32[]{:S(2)}) copy-start(bf16[256,512]{1,0:T(8,128)(2,1)} %param.17) | copy-start | bytes 786436
  39.2 59.6 %all-gather.8.cloned.1.call-start = ((), (), s32[]{:S(2)}) async-start(), calls=%async_computation.5 | async-start | bytes 3932160 | tf_op jit(solution)/shard_map/all_gather | solution.py:146
  63.7 113.5 %all-gather.10.cloned.1.call-start = ((), (), s32[]{:S(2)}) async-start(), calls=%async_computation.6 | async-start | bytes 2359296 | tf_op jit(solution)/shard_map/all_gather | solution.py:148
  64.3 7.9 %collective-permute-start = (bf16[1,256,512]{2,1,0:T(8,128)(2,1)S(1)}, bf16[1,256,512]{2,1,0:T(8,128)(2,1)S(1)}, u32[]{:S(2)}, u32[]{:S(2)}) collective-permute-start(bf16[1,256,512]{2,1,0:T(8,128)(2,1)S(1)} %convert_bitcast_fusion.1), channel_id=1, source_target_pairs={{0,4},{4,8},{8,12},{12,16},{16,20},{20,24},{24,28},{1,5},{5,9},{9,... | collective-permute-start | bytes 786440 | tf_op jit(solution)/shard_map/ppermute | solution.py:20
  73.0 8.8 %collective-permute-start.1 = (bf16[1,256,512]{2,1,0:T(8,128)(2,1)}, bf16[1,256,512]{2,1,0:T(8,128)(2,1)S(1)}, u32[]{:S(2)}, u32[]{:S(2)}) collective-permute-start(bf16[1,256,512]{2,1,0:T(8,128)(2,1)} %fusion.56), channel_id=1, source_target_pairs={{0,8},{4,12},{8,16},{12,20},{16,24},{20,28},{1,9},{5,13},{9,17},{1... | collective-permute-start | bytes 786440 | tf_op jit(solution)/shard_map/ppermute | solution.py:20
  82.6 9.3 %collective-permute-start.2 = (bf16[1,256,512]{2,1,0:T(8,128)(2,1)}, bf16[1,256,512]{2,1,0:T(8,128)(2,1)S(1)}, u32[]{:S(2)}, u32[]{:S(2)}) collective-permute-start(bf16[1,256,512]{2,1,0:T(8,128)(2,1)} %fusion.48), channel_id=1, source_target_pairs={{0,16},{4,20},{8,24},{12,28},{1,17},{5,21},{9,25},{13,29},{2,18},{... | collective-permute-start | bytes 786440 | tf_op jit(solution)/shard_map/ppermute | solution.py:20
  98.8 4.6 %copy-start.6 = (bf16[1,2048,256]{2,1,0:T(8,128)(2,1)S(1)}, bf16[1,2048,256]{2,1,0:T(8,128)(2,1)}, u32[]{:S(2)}) copy-start(bf16[1,2048,256]{2,1,0:T(8,128)(2,1)} %param.20) | copy-start | bytes 3145732
  114.2 2.5 collective-permute-start.4
  114.2 5.4 %collective-permute-start.3 = (bf16[1,768,512]{2,1,0:T(8,128)(2,1)}, bf16[1,768,512]{2,1,0:T(8,128)(2,1)S(1)}, u32[]{:S(2)}, u32[]{:S(2)}) collective-permute-start(bf16[1,768,512]{2,1,0:T(8,128)(2,1)} %get-tuple-element.64), channel_id=1, source_target_pairs={{0,1},{1,0},{2,3},{3,2},{4,5},{5,4},{6,7},{7,6},{8,9},{9,8},{10,11... | collective-permute-start | bytes 2359304 | tf_op jit(solution)/shard_map/ppermute | solution.py:41
  118.1 19.6 %collective-permute-start.5 = (bf16[1,768,512]{2,1,0:T(8,128)(2,1)S(1)}, bf16[1,768,512]{2,1,0:T(8,128)(2,1)S(1)}, u32[]{:S(2)}, u32[]{:S(2)}) collective-permute-start(bf16[1,768,512]{2,1,0:T(8,128)(2,1)S(1)} %add_convert_fusion.2), channel_id=1, source_target_pairs={{0,2},{1,3},{2,0},{3,1},{4,6},{5,7},{6,4},{7,5},{8,10},{9,11},{10,... | collective-permute-start | bytes 2359304 | tf_op jit(solution)/shard_map/ppermute | solution.py:41
  140.1 37.1 %all-to-all-start.2 = ((bf16[8,1,96,512]{3,2,1,0:T(8,128)(2,1)}), bf16[8,1,96,512]{3,2,1,0:T(8,128)(2,1)S(1)}, u32[]{:S(2)}, u32[]{:S(2)}) async-start(bf16[8,1,96,512]{3,2,1,0:T(8,128)(2,1)} %bitcast.166), calls=%async_computation.2 | async-start | bytes 1572864 | tf_op jit(solution)/shard_map/all_to_all | solution.py:155
  150.4 43.1 %all-gather.12.cloned.1.call-start = ((), (), s32[]{:S(2)}) async-start(), calls=%async_computation.7 | async-start | bytes 1310720 | tf_op jit(solution)/shard_map/all_gather | solution.py:164
  178.5 4.5 %copy-start.13 = (bf16[1,768,2048]{2,1,0:T(8,128)(2,1)S(1)}, bf16[1,768,2048]{2,1,0:T(8,128)(2,1)}, u32[]{:S(2)}) copy-start(bf16[1,768,2048]{2,1,0:T(8,128)(2,1)} %all-gather.8.cloned.1.call-done) | copy-start | bytes 9437188
  185.3 17.9 %copy-start.4 = (bf16[256,256]{1,0:T(8,128)(2,1)S(1)}, bf16[256,256]{1,0:T(8,128)(2,1)}, u32[]{:S(2)}) copy-start(bf16[256,256]{1,0:T(8,128)(2,1)} %param.15) | copy-start | bytes 393220
  195.4 21.1 %all-to-all-start.3 = ((bf16[8,64,256]{2,1,0:T(8,128)(2,1)}), bf16[8,64,256]{2,1,0:T(8,128)(2,1)}, u32[]{:S(2)}, u32[]{:S(2)}) async-start(bf16[8,64,256]{2,1,0:T(8,128)(2,1)} %copy.43), calls=%async_computation.3 | async-start | bytes 524288 | tf_op jit(solution)/shard_map/all_to_all | solution.py:171
  200.9 48.2 %all-gather.14.cloned.1.call-start = ((), (), s32[]{:S(2)}) async-start(), calls=%async_computation.8 | async-start | bytes 1310720 | tf_op jit(solution)/shard_map/all_gather | solution.py:172
  203.6 10.8 %collective-permute-start.6 = (bf16[1,256,512]{2,1,0:T(8,128)(2,1)S(1)}, bf16[1,256,512]{2,1,0:T(8,128)(2,1)S(1)}, u32[]{:S(2)}, u32[]{:S(2)}) collective-permute-start(bf16[1,256,512]{2,1,0:T(8,128)(2,1)S(1)} %convert_bitcast_fusion), channel_id=1, source_target_pairs={{4,0},{8,4},{12,8},{16,12},{20,16},{24,20},{28,24},{5,1},{9,5},{13... | collective-permute-start | bytes 786440 | tf_op jit(solution)/shard_map/ppermute | solution.py:20
  215.2 9.9 %collective-permute-start.7 = (bf16[1,256,512]{2,1,0:T(8,128)(2,1)}, bf16[1,256,512]{2,1,0:T(8,128)(2,1)}, u32[]{:S(2)}, u32[]{:S(2)}) collective-permute-start(bf16[1,256,512]{2,1,0:T(8,128)(2,1)} %fusion.55), channel_id=1, source_target_pairs={{8,0},{12,4},{16,8},{20,12},{24,16},{28,20},{9,1},{13,5},{17,9},{2... | collective-permute-start | bytes 786440 | tf_op jit(solution)/shard_map/ppermute | solution.py:20
  226.9 15.4 %collective-permute-start.8 = (bf16[1,256,512]{2,1,0:T(8,128)(2,1)}, bf16[1,256,512]{2,1,0:T(8,128)(2,1)}, u32[]{:S(2)}, u32[]{:S(2)}) collective-permute-start(bf16[1,256,512]{2,1,0:T(8,128)(2,1)} %fusion.54), channel_id=1, source_target_pairs={{16,0},{20,4},{24,8},{28,12},{17,1},{21,5},{25,9},{29,13},{18,2},{... | collective-permute-start | bytes 786440 | tf_op jit(solution)/shard_map/ppermute | solution.py:20
  (9 other events, 28.9 us)
Sparse Core Ops, SparseCore 0:
  39.3 27.4 all-gather.5
  68.4 28.4 all-gather.7
  107.3 67.6 all-gather.9
  178.5 15.0 all-gather.11
  218.4 18.6 all-gather.13
where the time goes:
time: 261 us; the launch traced here: 260 us
  waiting for transfers between devices  110 us (42%)
  matrix products  45.2 us (17%)
  starting transfers between devices  42.6 us (16%)
  blocking collectives  23.8 us (9%)
  between operations  14.5 us (6%)
  local copies, waits for them, and re-layouts  13.4 us (5%)
  other arithmetic  10.5 us (4%)
    ppermute x6, waiting for transfers between devices, carried(): lax.ppermute(held.astype(jnp.bfloat16), axis, pairs).astype(jnp.float32)  36.1 us
    all_to_all x1, waiting for transfers between devices, local(): lax.all_to_all(row_grad, 'sp', split_axis=0, concat_axis=0, tiled=True)  26.6 us
    all_to_all x1, blocking collectives, to_experts(): return lax.all_to_all(rows, 'sp', split_axis=0, concat_axis=1, tiled=True)  23.8 us
    ppermute x3, waiting for transfers between devices, scattered_sum(): got = lax.ppermute(pieces.pop(k), axis, pairs)  20.1 us
    all_to_all x1, waiting for transfers between devices, to_experts(): return lax.all_to_all(rows, 'sp', split_axis=0, concat_axis=1, tiled=True)  19.1 us
    ppermute x6, starting transfers between devices, carried(): lax.ppermute(held.astype(jnp.bfloat16), axis, pairs).astype(jnp.float32)  16.9 us
    all_to_all x1, starting transfers between devices, local(): lax.all_to_all(row_grad, 'sp', split_axis=0, concat_axis=0, tiled=True)  10.4 us
    all_gather x1, waiting for transfers between devices, local(): layer_grad = lax.all_gather(layer_cols, 'tp', axis=1, tiled=True)  8.23 us
  transfers between devices with their start and end apart: 17, of which 11 were waited for; matrix products, arithmetic and copies ran while one was open for 18% of the time, Pallas kernels for 0%

commit v1 on v0

v1 whole, which is shorter than its diff:
```python
import functools
import math

import jax
import jax.numpy as jnp
from jax import lax
from jax.experimental import pallas as pl
from jax.experimental.pallas import tpu as pltpu
from jax.sharding import PartitionSpec as P

H = 4
DK = 256
DV = 512
GROUPS = 4
MESH = pl.DeviceIdType.MESH
ROWS = (((0,), (0,)), ((), ()))
COLS = (((1,), (1,)), ((), ()))


def dot(a, b, dims=(((1,), (0,)), ((), ()))):
    return lax.dot_general(a, b, dims, preferred_element_type=jnp.float32)


def carried(part, log_span, axis, reverse):
    count = lax.axis_size(axis)
    held = part
    ahead = jnp.zeros_like(part)
    step = 1
    while step < count:
        pairs = [(i + step, i) if reverse else (i, i + step) for i in range(count - step)]
        got = lax.ppermute(held.astype(jnp.bfloat16), axis, pairs).astype(jnp.float32)
        ahead = ahead + jnp.exp(log_span * (step - 1.0))[:, None, None] * got
        held = held + jnp.exp(log_span * float(step))[:, None, None] * got
        step *= 2
    return ahead


def moe_kernel(
    count,
    place_ref,
    rw_ref,
    hid_ref,
    cot_ref,
    wg_hbm,
    wu_hbm,
    wd_hbm,
    layer_out,
    gg_ref,
    ug_ref,
    dg_ref,
    wg,
    wu,
    wd,
    packed,
    packed2,
    got,
    terms,
    part,
    half,
    kept,
    moving,
    other,
    ret,
    total,
    layer,
    wsem,
    d_s,
    d_r,
    a_s,
    a_r,
    b_s,
    b_r,
    c_s,
    c_r,
    h_s,
    h_r,
    x_s,
    x_r,
    r_s,
    r_r,
    la_s,
    la_r,
    lb_s,
    lb_r,
    lc_s,
    lc_r,
):
    sp = lax.axis_index("sp")
    tp = lax.axis_index("tp")
    cap = place_ref.shape[1]
    wide = hid_ref.shape[1] // 4
    per = count // GROUPS
    offs = [pl.multiple_of(jnp.bitwise_xor(tp, r) * wide, wide) for r in range(4)]
    cols = [pl.ds(o, wide) for o in offs]

    loads = [
        pltpu.make_async_copy(src, dst, wsem.at[i])
        for i, (src, dst) in enumerate(((wg_hbm, wg), (wu_hbm, wu), (wd_hbm, wd)))
    ]
    for load in loads:
        load.start()

    def along_sp(m, src, dst, s, r):
        peer = (jnp.bitwise_xor(sp, m), tp)
        return pltpu.make_async_remote_copy(src, dst, s, r, device_id=peer, device_id_type=MESH)

    def along_tp(m, src, dst, s, r):
        peer = (sp, jnp.bitwise_xor(tp, m))
        return pltpu.make_async_remote_copy(src, dst, s, r, device_id=peer, device_id_type=MESH)

    barrier = pltpu.get_barrier_semaphore()
    for m in range(1, count):
        pl.semaphore_signal(
            barrier, inc=1, device_id=(jnp.bitwise_xor(sp, m), tp), device_id_type=MESH
        )
    for m in (1, 2):
        pl.semaphore_signal(
            barrier, inc=1, device_id=(sp, jnp.bitwise_xor(tp, m)), device_id_type=MESH
        )

    def pack(m, r):
        one = place_ref[jnp.bitwise_xor(sp, m)]
        rows = dot(one, hid_ref[:, cols[r]]).astype(jnp.bfloat16)
        ups = rw_ref[jnp.bitwise_xor(sp, m)] * dot(one, cot_ref[:, cols[r]])
        return rows, ups.astype(jnp.bfloat16)

    def stored(ref, pair):
        ref[0], ref[1] = pair

    sends = []

    def begin(copy):
        copy.start()
        sends.append(copy)
        return copy

    stored(packed.at[1], pack(1, 0))
    stored(packed2, pack(1, 2))
    pl.semaphore_wait(barrier, count + 1)
    arrive = {}
    arrive2 = begin(along_sp(1, packed2, got.at[2, :, 1], d_s.at[0], d_r.at[0]))
    for m in range(1, count):
        if m > 1:
            stored(packed.at[m], pack(m, 0))
        arrive[m] = begin(along_sp(m, packed.at[m], got.at[0, :, m], d_s.at[m], d_r.at[m]))
    for r in range(4):
        rows, ups = pack(0, r)
        got[r, 0, 0] = rows
        got[r, 1, 0] = ups

    from_pair, from_x, from_diag = {}, {}, {}

    def relay_first(m):
        arrive[m].wait_recv()
        from_pair[m] = begin(along_tp(1, got.at[0, :, m], got.at[1, :, m], a_s.at[m], a_r.at[m]))
        if m > 1:
            from_x[m] = begin(along_tp(2, got.at[0, :, m], got.at[2, :, m], b_s.at[m], b_r.at[m]))

    def relay_second(m):
        if m > 1:
            from_x[m].wait_recv()
        else:
            arrive2.wait_recv()
        from_diag[m] = begin(along_tp(1, got.at[2, :, m], got.at[3, :, m], c_s.at[m], c_r.at[m]))

    def rows_of(a, r, g):
        return got[r, a, g * per : (g + 1) * per].reshape(per * cap, wide)

    halves, across = {}, {}
    n = per * cap

    def expert(g):
        for m in range(max(1, g * per), (g + 1) * per):
            from_pair[m].wait_recv()
            from_diag[m].wait_recv()
        gate_pre = sum(dot(rows_of(0, r, g), wg[cols[r], :]) for r in range(4))
        up_pre = sum(dot(rows_of(0, r, g), wu[cols[r], :]) for r in range(4))
        unit = sum(dot(rows_of(1, r, g), wd[:, cols[r]], COLS) for r in range(4))
        sigma = jax.nn.sigmoid(gate_pre)
        active = gate_pre * sigma
        span = pl.ds(g * n, n)
        terms[0, span] = (active * up_pre).astype(jnp.bfloat16)
        gate_term = (unit * up_pre * sigma * (1.0 + gate_pre * (1.0 - sigma))).astype(jnp.bfloat16)
        up_term = (unit * active).astype(jnp.bfloat16)
        terms[1, span] = gate_term
        terms[2, span] = up_term
        for at, r in ((2, 1), (3, 3), (0, 0), (1, 2)):
            piece = dot(gate_term, wg[cols[r], :], COLS) + dot(up_term, wu[cols[r], :], COLS)
            part[at, span] = piece.astype(jnp.bfloat16)
            if at == 3:
                halves[g] = begin(
                    along_tp(1, part.at[2:4, span], half.at[:, span], h_s.at[g], h_r.at[g])
                )

    def cross(g):
        span = pl.ds(g * n, n)
        halves[g].wait_recv()
        mine = part[1, span].astype(jnp.float32) + half[1, span].astype(jnp.float32)
        moving[span] = mine.astype(jnp.bfloat16)
        across[g] = begin(along_tp(2, moving.at[span], other.at[span], x_s.at[g], x_r.at[g]))
        mine = part[0, span].astype(jnp.float32) + half[0, span].astype(jnp.float32)
        kept[span] = mine.astype(jnp.bfloat16)

    back = {}

    def give_back(g):
        across[g].wait_recv()
        for m in range(g * per, (g + 1) * per):
            span = pl.ds(m * cap, cap)
            done = kept[span].astype(jnp.float32) + other[span].astype(jnp.float32)
            if m == 0:
                ret[0] = done.astype(jnp.bfloat16)
            else:
                kept[span] = done.astype(jnp.bfloat16)
                back[m] = begin(along_sp(m, kept.at[span], ret.at[m], r_s.at[m], r_r.at[m]))

    for m in range(1, per):
        relay_first(m)
        relay_second(m)
    for load in loads:
        load.wait()
    for g in range(1, GROUPS):
        for m in range(g * per, (g + 1) * per):
            relay_first(m)
            if m > g * per:
                relay_second(m - 1)
        expert(g - 1)
        relay_second((g + 1) * per - 1)
        cross(g - 1)
        if g > 1:
            give_back(g - 2)
    expert(GROUPS - 1)
    give_back(GROUPS - 2)
    cross(GROUPS - 1)

    def whole(a, r):
        return got[r, a].reshape(count * cap, wide)

    for r in range(4):
        dg_ref[:, cols[r]] = dot(terms[0], whole(1, r), ROWS)
    give_back(GROUPS - 1)
    for r in range(4):
        gg_ref[cols[r], :] = dot(whole(0, r), terms[1], ROWS)
        ug_ref[cols[r], :] = dot(whole(0, r), terms[2], ROWS)
    total[...] = cot_ref[:, cols[0]].astype(jnp.float32)
    for m in range(count):
        if m:
            back[m].wait_recv()
        total[...] += dot(place_ref[jnp.bitwise_xor(sp, m)], ret[m], ROWS)
    layer[0] = total[...].astype(jnp.bfloat16)
    one = begin(along_tp(2, layer.at[0], layer.at[2], lb_s, lb_r))
    two = begin(along_tp(1, layer.at[0], layer.at[1], la_s, la_r))
    one.wait_recv()
    three = begin(along_tp(1, layer.at[2], layer.at[3], lc_s, lc_r))
    two.wait_recv()
    three.wait_recv()
    for r in range(4):
        layer_out[:, cols[r]] = layer[r]
    for copy in sends:
        copy.wait_send()


def moe(place, row_weight, hidden, cotangent, gate_w, up_w, down_w):
    count = lax.axis_size("sp")
    assert lax.axis_size("tp") == 4 and count % GROUPS == 0
    experts, cap, tokens = place.shape
    width = hidden.shape[1]
    units = gate_w.shape[1]
    wide = width // 4
    rows = count * cap
    bf, f32 = jnp.bfloat16, jnp.float32
    dma = pltpu.SemaphoreType.DMA
    vmem = pl.BlockSpec(memory_space=pltpu.VMEM)
    hbm = pl.BlockSpec(memory_space=pl.ANY)
    return pl.pallas_call(
        functools.partial(moe_kernel, count),
        out_shape=(
            jax.ShapeDtypeStruct((tokens, width), bf),
            jax.ShapeDtypeStruct((width, units), f32),
            jax.ShapeDtypeStruct((width, units), f32),
            jax.ShapeDtypeStruct((units, width), f32),
        ),
        in_specs=[vmem] * 4 + [hbm] * 3,
        out_specs=(vmem,) * 4,
        scratch_shapes=[
            pltpu.VMEM((width, units), bf),
            pltpu.VMEM((width, units), bf),
            pltpu.VMEM((units, width), bf),
            pltpu.VMEM((count, 2, cap, wide), bf),
            pltpu.VMEM((2, cap, wide), bf),
            pltpu.VMEM((4, 2, count, cap, wide), bf),
            pltpu.VMEM((3, rows, units), bf),
            pltpu.VMEM((4, rows, wide), bf),
            pltpu.VMEM((2, rows, wide), bf),
            pltpu.VMEM((rows, wide), bf),
            pltpu.VMEM((rows, wide), bf),
            pltpu.VMEM((rows, wide), bf),
            pltpu.VMEM((count, cap, wide), bf),
            pltpu.VMEM((tokens, wide), f32),
            pltpu.VMEM((4, tokens, wide), bf),
            dma((3,)),
        ]
        + [dma((count,))] * 8
        + [dma((GROUPS,))] * 4
        + [dma((count,))] * 2
        + [dma] * 6,
        compiler_params=pltpu.CompilerParams(
            collective_id=0, has_side_effects=True, vmem_limit_bytes=60 * 2**20
        ),
        name="moe",
    )(place, row_weight, hidden, cotangent, gate_w, up_w, down_w)


def head_rates(head_ids, total_tokens):
    ids = head_ids.astype(jnp.float32)
    exponent = jnp.where(2 * head_ids < H, -5.0 - ids, -math.log2(total_tokens) - (ids - H // 2))
    log_gamma = jnp.log1p(-jnp.exp2(exponent))
    scale = jnp.sqrt(-jnp.expm1(2.0 * log_gamma))
    return (log_gamma, scale)


def routing(routes, route_weight, experts_all, tok_local):
    top_count = routes.shape[1]
    capacity = 3 * tok_local * top_count // (2 * experts_all)
    capacity = -(-capacity // 16) * 16
    ids = jnp.arange(experts_all, dtype=jnp.int32)[:, None]
    named = [routes[:, r][None, :] == ids for r in range(top_count)]
    member = sum(m.astype(jnp.float32) for m in named)
    slot_weight = sum(jnp.where(m, route_weight[:, r][None, :], 0.0) for r, m in enumerate(named))
    order = jnp.arange(tok_local, dtype=jnp.int32)
    earlier = (order[:, None] < order[None, :]).astype(jnp.bfloat16)
    rank = jnp.dot(member.astype(jnp.bfloat16), earlier, preferred_element_type=jnp.float32)
    rank = jnp.where(member > 0.0, rank, -1.0).astype(jnp.int32)
    hit = rank[:, None, :] == jnp.arange(capacity, dtype=jnp.int32)[None, :, None]
    row_weight = jnp.sum(jnp.where(hit, slot_weight[:, None, :], 0.0), axis=2, keepdims=True)
    return hit.astype(jnp.bfloat16), row_weight


def local(
    hidden,
    cotangent,
    retained,
    queries,
    key_rows,
    value_rows,
    routes,
    route_weight,
    gate_weight,
    up_weight,
    down_weight,
    out_weight,
):
    sp_count = lax.axis_size("sp")
    tp_count = lax.axis_size("tp")
    tok_local = hidden.shape[0]
    experts_all = gate_weight.shape[0] * sp_count
    assert gate_weight.shape[0] == 1
    place_rows, row_weight = routing(routes, route_weight, experts_all, tok_local)
    heads_local = queries.shape[1] // DK
    head_ids = lax.axis_index("tp") * heads_local + jnp.arange(heads_local, dtype=jnp.int32)
    log_gamma, scale = head_rates(head_ids, tok_local * sp_count)
    query_three = queries.reshape(tok_local, heads_local, DK)
    key_three = key_rows.reshape(tok_local, heads_local, DK)
    value_three = value_rows.reshape(tok_local, heads_local, DV)
    place = jnp.arange(tok_local, dtype=jnp.float32)
    suffix_decay = jnp.exp(log_gamma[None, :] * (tok_local - place[:, None]))
    prefix_decay = jnp.exp(log_gamma[None, :] * (place[:, None] + 1.0))
    forward_shard_local = jnp.einsum(
        "ibz,ibm->bzm",
        (key_three * suffix_decay[:, :, None]).astype(jnp.bfloat16),
        value_three,
        preferred_element_type=jnp.float32,
    )
    log_span = log_gamma * tok_local
    retained_all = lax.all_gather(retained, "sp", axis=0, tiled=True)
    layer_grad, gate_grad, up_grad, down_grad = moe(
        place_rows,
        row_weight,
        hidden,
        cotangent,
        gate_weight[0],
        up_weight[0],
        down_weight[0],
    )
    prior_positions = carried(forward_shard_local, log_span, "sp", False).astype(jnp.bfloat16)
    mixed_grad = jnp.dot(layer_grad, out_weight, preferred_element_type=jnp.float32).astype(
        jnp.bfloat16
    )
    share = tok_local // tp_count
    share_rows = lax.dynamic_slice_in_dim(layer_grad, lax.axis_index("tp") * share, share, 0)
    share_rows = share_rows.reshape(share, sp_count, -1).swapaxes(0, 1)
    block_rows = lax.all_to_all(share_rows, "sp", split_axis=0, concat_axis=0, tiled=True)
    block_all = lax.all_gather(block_rows, "tp", axis=1, tiled=True)
    proj_grad = lax.dot_general(
        block_all.reshape(sp_count * tok_local, -1),
        retained_all,
        (((0,), (0,)), ((), ())),
        preferred_element_type=jnp.float32,
    )
    output_grad_three = mixed_grad.reshape(tok_local, heads_local, DV)
    backward_local = jnp.einsum(
        "stz,stb->tzb",
        (query_three * prefix_decay[:, :, None]).astype(jnp.bfloat16),
        output_grad_three,
        preferred_element_type=jnp.float32,
    )
    later_positions = carried(backward_local, log_span, "sp", True).astype(jnp.bfloat16)
    gap = place[:, None] - place[None, :]
    weight = jnp.where(
        gap[None] >= 0,
        scale[:, None, None] * jnp.exp(log_gamma[:, None, None] * jnp.maximum(gap, 0.0)[None]),
        0.0,
    )
    local_value_grad = (
        jnp.einsum(
            "ihv,jhv->hij", output_grad_three, value_three, preferred_element_type=jnp.float32
        )
        * weight
    ).astype(jnp.bfloat16)
    local_query_key = (
        jnp.einsum("ihd,jhd->hij", query_three, key_three, preferred_element_type=jnp.float32)
        * weight
    ).astype(jnp.bfloat16)
    leading_span = (scale[None, :] * jnp.exp(log_gamma[None, :] * place[:, None]))[:, :, None]
    trailing_span = (
        scale[None, :] * jnp.exp(log_gamma[None, :] * (tok_local - 1.0 - place[:, None]))
    )[:, :, None]
    query_gradient = jnp.einsum(
        "zby,yze->bze", local_value_grad, key_three, preferred_element_type=jnp.float32
    )
    query_gradient = query_gradient + leading_span * jnp.einsum(
        "eal,gel->gea", prior_positions, output_grad_three, preferred_element_type=jnp.float32
    )
    key_gradient = jnp.einsum(
        "lcx,clo->xlo", local_value_grad, query_three, preferred_element_type=jnp.float32
    )
    key_gradient = key_gradient + trailing_span * jnp.einsum(
        "gta,wga->wgt", later_positions, value_three, preferred_element_type=jnp.float32
    )
    value_gradient = jnp.einsum(
        "upb,puk->buk", local_query_key, output_grad_three, preferred_element_type=jnp.float32
    )
    value_gradient = value_gradient + trailing_span * jnp.einsum(
        "tdx,btd->btx", later_positions, key_three, preferred_element_type=jnp.float32
    )
    return (
        gate_grad[None],
        up_grad[None],
        down_grad[None],
        proj_grad,
        query_gradient.reshape(tok_local, heads_local * DK),
        key_gradient.reshape(tok_local, heads_local * DK),
        value_gradient.reshape(tok_local, heads_local * DV),
    )


def solution(mesh):
    return jax.shard_map(
        local,
        mesh=mesh,
        in_specs=(
            P("sp", None),
            P("sp", None),
            P("sp", "tp"),
            P("sp", "tp"),
            P("sp", "tp"),
            P("sp", "tp"),
            P("sp", None),
            P("sp", None),
            P("sp", None, "tp"),
            P("sp", None, "tp"),
            P("sp", "tp", None),
            P(None, "tp"),
        ),
        out_specs=(
            P("sp", None, "tp"),
            P("sp", None, "tp"),
            P("sp", "tp", None),
            P("sp", "tp"),
            P("sp", "tp"),
            P("sp", "tp"),
            P("sp", "tp"),
        ),
        check_vma=False,
    )
```

time: 261 us -> 213 us (0.82)
  Pallas kernels: 0 us -> 93.6 us
  waiting for transfers between devices: 110 us -> 26.6 us
  matrix products: 45.2 us -> 18.1 us
  starting transfers between devices: 42.6 us -> 20.5 us
  blocking collectives: 23.8 us -> 16.3 us
    pallas_call x0 -> x1, Pallas kernels: none -> 93.6 us  [moe(): pl.pallas_call(functools.partial(moe_kernel, count), out_shape=(jax.Shape...]
    all_to_all x3 -> x0, waiting for transfers between devices: 45.8 us -> none  [the longest x1 26.6 us: local(): lax.all_to_all(row_grad, 'sp', split_axis=0, concat_axis=0, tiled=True)]
    dot_general x12 -> x1, matrix products: 31.9 us -> 0.15 us  [routing(): jnp.dot(member.astype(jnp.bfloat16), earlier, preferred_element_type=jnp....]
    ppermute x6, waiting for transfers between devices: 36.1 us -> 11.6 us  [carried(): lax.ppermute(held.astype(jnp.bfloat16), axis, pairs).astype(jnp.float32)]
    all_to_all x3 -> x0, starting transfers between devices: 23.3 us -> none  [the longest x1 10.4 us: local(): lax.all_to_all(row_grad, 'sp', split_axis=0, concat_axis=0, tiled=True)]
    ppermute x3 -> x0, waiting for transfers between devices: 20.1 us -> none  [scattered_sum(): got = lax.ppermute(pieces.pop(k), axis, pairs)]
    all_gather x1, waiting for transfers between devices: 0.01 us -> 14.4 us  [local(): retained_all = lax.all_gather(retained, 'sp', axis=0, tiled=True)]
    all_gather x3 -> x0, waiting for transfers between devices: 8.23 us -> none  [the longest x1 8.23 us: local(): layer_grad = lax.all_gather(layer_cols, 'tp', axis=1, tiled=True)]
  transfers between devices with their start and end apart: 17 -> 8, of which waited for: 11 -> 3; matrix products, arithmetic and copies ran while one was open for 18% -> 12% of each run, Pallas kernels for 0% -> 0%
where the time goes in v1:
time: 213 us
  Pallas kernels  93.6 us (44%)
  waiting for transfers between devices  26.6 us (12%)
  starting transfers between devices  20.5 us (10%)
  matrix products  18.1 us (8%)
  blocking collectives  16.3 us (8%)
  between operations  14.6 us (7%)
  local copies, waits for them, and re-layouts  13.2 us (6%)
  other arithmetic  9.8 us (5%)
    pallas_call x1, Pallas kernels, moe(): pl.pallas_call(functools.partial(moe_kernel, count), out_shape=(jax.Shape...  93.6 us
    ppermute x6, starting transfers between devices, carried(): lax.ppermute(held.astype(jnp.bfloat16), axis, pairs).astype(jnp.float32)  20.2 us
    all_to_all x1, blocking collectives, local(): lax.all_to_all(share_rows, 'sp', split_axis=0, concat_axis=0, tiled=True)  16.3 us
    all_gather x1, waiting for transfers between devices, local(): retained_all = lax.all_gather(retained, 'sp', axis=0, tiled=True)  14.4 us
    ppermute x6, waiting for transfers between devices, carried(): lax.ppermute(held.astype(jnp.bfloat16), axis, pairs).astype(jnp.float32)  11.6 us
    convert_element_type x6, other arithmetic, carried(): held.astype(jnp.bfloat16)  7.6 us
    unnamed x23, local copies, waits for them, and re-layouts  7.34 us
  transfers between devices with their start and end apart: 8, of which 3 were waited for; matrix products, arithmetic and copies ran while one was open for 12% of the time, Pallas kernels for 0%

profile of v1, /device:TPU:0, one launch (start us, length us, event | category | flops | bytes accessed | tf_op | source)
XLA Modules:
  0.0 212.6 jit_solution(8059360483412109901)
XLA Ops:
  11.0 93.6 %moe.1 = (bf16[256,2048]{1,0:T(8,128)(2,1)}, f32[2048,256]{1,0:T(8,128)}, f32[2048,256]{1,0:T(8,128)}, f32[256,2048]{1,0:T(8,128)}) custom-call(bf16[8,96,256]{2,1,0:T(8,128)(2,1)} %fusion.12.place_ref, f32[8,96,1]{2,1,0:T(8,128)} %copy.28.rw_ref, bf16[256,2048]{1,0:T(8,128)(2,1)} %hid_ref.1, bf16[256,2048]{1,0:T(8,128)(2,1)} %cot_ref.1, ...), custom_call_target="tpu_custom_call" | custom-call | tf_op jit(solution)/shard_map/moe/pallas_call | solution.py:275
  105.7 16.3 %all_to_all.5 = bf16[8,64,256]{2,1,0:T(8,128)(2,1)S(1)} all-to-all(bf16[8,64,256]{2,1,0:T(8,128)(2,1)S(1)} %copy.29), channel_id=1, replica_groups=mesh['sp'=8,'tp'=4] {'sp'}, dimensions={0} | all-to-all | bytes 524288 | tf_op jit(solution)/shard_map/all_to_all | solution.py:392
  123.7 2.0 convolution_convert_fusion
  127.1 1.3 collective-permute-start.3
  128.4 1.3 fusion.35
  130.4 5.2 %collective-permute-start = (bf16[1,256,512]{2,1,0:T(8,128)(2,1)}, bf16[1,256,512]{2,1,0:T(8,128)(2,1)}, u32[]{:S(2)}, u32[]{:S(2)}) collective-permute-start(bf16[1,256,512]{2,1,0:T(8,128)(2,1)} %convert_bitcast_fusion.1), channel_id=1, source_target_pairs={{0,4},{4,8},{8,12},{12,16},{16,20},{20,24},{24,28},{1,5},{5,9},{9,... | collective-permute-start | bytes 786440 | tf_op jit(solution)/shard_map/ppermute | solution.py:31
  135.8 1.3 fusion.9
  137.1 1.8 convolution_bitcast_fusion.1
  141.9 1.7 fusion.26
  143.7 5.2 %collective-permute-start.1 = (bf16[1,256,512]{2,1,0:T(8,128)(2,1)}, bf16[1,256,512]{2,1,0:T(8,128)(2,1)}, u32[]{:S(2)}, u32[]{:S(2)}) collective-permute-start(bf16[1,256,512]{2,1,0:T(8,128)(2,1)} %fusion.26), channel_id=1, source_target_pairs={{0,8},{4,12},{8,16},{12,20},{16,24},{20,28},{1,9},{5,13},{9,17},{1... | collective-permute-start | bytes 786440 | tf_op jit(solution)/shard_map/ppermute | solution.py:31
  148.9 1.8 fusion.24
  152.1 6.4 %collective-permute-done.1 = bf16[1,256,512]{2,1,0:T(8,128)(2,1)} collective-permute-done((bf16[1,256,512]{2,1,0:T(8,128)(2,1)}, bf16[1,256,512]{2,1,0:T(8,128)(2,1)}, u32[]{:S(2)}, u32[]{:S(2)}) %collective-permute-start.1) | collective-permute-done | bytes 262176 | tf_op jit(solution)/shard_map/ppermute | solution.py:31
  158.5 1.9 fusion.18
  160.4 5.9 %collective-permute-start.2 = (bf16[1,256,512]{2,1,0:T(8,128)(2,1)}, bf16[1,256,512]{2,1,0:T(8,128)(2,1)}, u32[]{:S(2)}, u32[]{:S(2)}) collective-permute-start(bf16[1,256,512]{2,1,0:T(8,128)(2,1)} %fusion.18), channel_id=1, source_target_pairs={{0,16},{4,20},{8,24},{12,28},{1,17},{5,21},{9,25},{13,29},{2,18},{... | collective-permute-start | bytes 786440 | tf_op jit(solution)/shard_map/ppermute | solution.py:31
  166.3 5.1 %collective-permute-done.5 = bf16[1,256,512]{2,1,0:T(8,128)(2,1)S(1)} collective-permute-done((bf16[1,256,512]{2,1,0:T(8,128)(2,1)}, bf16[1,256,512]{2,1,0:T(8,128)(2,1)S(1)}, u32[]{:S(2)}, u32[]{:S(2)}) %collective-permute-start.5) | collective-permute-done | bytes 262176 | tf_op jit(solution)/shard_map/ppermute | solution.py:31
  173.6 1.8 fusion.2
  176.4 1.9 fusion.8
  178.4 2.2 %fusion.6 = f32[256,256]{1,0:T(8,128)} fusion(f32[256,1,256]{2,0,1:T(8,128)} %convolution_bitcast_fusion.2, bf16[256,512]{1,0:T(8,128)(2,1)S(1)} %copy-done.2, bf16[1,256,512]{2,1,0:T(8,128)(2,1)} %collective-permute-done.2, bf16[1,256,512]{2,1,0:T(8,128)(2,1)} %collective-permute-done.1, bf16[1,256,512]{2,1,0:T(8,128)(2,1)} %collective-permute-done, ...), kind=kOutput, calls=%fused_computation.15 | convolution fusion | flops 68419584 | bytes 1573900 | tf_op jit(solution)/shard_map/eal,gel->gea/dot_general | solution.py:431
  180.6 1.4 copy.31
  182.0 14.4 %all-gather.5.cloned.1.call-done = bf16[2048,512]{1,0:T(8,128)(2,1)} async-done(((bf16[256,512]{1,0:T(8,128)(2,1)}), bf16[2048,512]{1,0:T(8,128)(2,1)}) %all-gather.5.cloned.1.call-update) | async-done | bytes 2097168 | tf_op jit(solution)/shard_map/all_gather | solution.py:375
  196.5 3.3 %fusion.50 = f32[256,512]{1,0:T(8,128)} fusion(bf16[2048,256]{1,0:T(8,128)(2,1)S(1)} %bitcast.105, bf16[2048,512]{1,0:T(8,128)(2,1)} %all-gather.5.cloned.1.call-done), kind=kOutput, calls=%fused_computation.83 | convolution fusion | flops 536870912 | bytes 3670016 | tf_op jit(solution)/shard_map/dot_general | solution.py:394
  199.8 1.3 copy.39
  202.1 1.3 copy.40
  204.5 1.3 copy.41
  (50 shorter events, 18.0 us)
Async XLA Ops:
  7.2 116.5 %copy-start = (bf16[2048,512]{1,0:T(8,128)(2,1)S(1)}, bf16[2048,512]{1,0:T(8,128)(2,1)}, u32[]{:S(2)}) copy-start(bf16[2048,512]{1,0:T(8,128)(2,1)} %param.23) | copy-start | bytes 6291460
  7.2 173.4 %all-gather.3.cloned.1.call-start = ((), (), s32[]{:S(2)}) async-start(), calls=%async_computation.1 | async-start | bytes 1310720 | tf_op jit(solution)/shard_map/all_gather | solution.py:393
  122.9 2.9 %copy-start.7 = (bf16[256,256]{1,0:T(8,128)(2,1)S(1)}, bf16[256,256]{1,0:T(8,128)(2,1)}, u32[]{:S(2)}) copy-start(bf16[256,256]{1,0:T(8,128)(2,1)} %param.15) | copy-start | bytes 393220
  122.9 73.6 %all-gather.5.cloned.1.call-start = ((), (), s32[]{:S(2)}) async-start(), calls=%async_computation.2 | async-start | bytes 2359296 | tf_op jit(solution)/shard_map/all_gather | solution.py:375
  123.6 4.7 %copy-start.6 = (bf16[256,256]{1,0:T(8,128)(2,1)S(1)}, bf16[256,256]{1,0:T(8,128)(2,1)}, u32[]{:S(2)}) copy-start(bf16[256,256]{1,0:T(8,128)(2,1)} %param.16) | copy-start | bytes 393220
  125.6 0.7 copy-start.1
  127.1 11.8 %collective-permute-start.3 = (bf16[1,256,512]{2,1,0:T(8,128)(2,1)}, bf16[1,256,512]{2,1,0:T(8,128)(2,1)S(1)}, u32[]{:S(2)}, u32[]{:S(2)}) collective-permute-start(bf16[1,256,512]{2,1,0:T(8,128)(2,1)} %convert_bitcast_fusion), channel_id=1, source_target_pairs={{4,0},{8,4},{12,8},{16,12},{20,16},{24,20},{28,24},{5,1},{9,5},{13... | collective-permute-start | bytes 786440 | tf_op jit(solution)/shard_map/ppermute | solution.py:31
  130.4 11.5 %collective-permute-start = (bf16[1,256,512]{2,1,0:T(8,128)(2,1)}, bf16[1,256,512]{2,1,0:T(8,128)(2,1)}, u32[]{:S(2)}, u32[]{:S(2)}) collective-permute-start(bf16[1,256,512]{2,1,0:T(8,128)(2,1)} %convert_bitcast_fusion.1), channel_id=1, source_target_pairs={{0,4},{4,8},{8,12},{12,16},{16,20},{20,24},{24,28},{1,5},{5,9},{9,... | collective-permute-start | bytes 786440 | tf_op jit(solution)/shard_map/ppermute | solution.py:31
  139.7 9.2 %collective-permute-start.4 = (bf16[1,256,512]{2,1,0:T(8,128)(2,1)}, bf16[1,256,512]{2,1,0:T(8,128)(2,1)}, u32[]{:S(2)}, u32[]{:S(2)}) collective-permute-start(bf16[1,256,512]{2,1,0:T(8,128)(2,1)} %fusion.25), channel_id=1, source_target_pairs={{8,0},{12,4},{16,8},{20,12},{24,16},{28,20},{9,1},{13,5},{17,9},{2... | collective-permute-start | bytes 786440 | tf_op jit(solution)/shard_map/ppermute | solution.py:31
  143.7 14.9 %collective-permute-start.1 = (bf16[1,256,512]{2,1,0:T(8,128)(2,1)}, bf16[1,256,512]{2,1,0:T(8,128)(2,1)}, u32[]{:S(2)}, u32[]{:S(2)}) collective-permute-start(bf16[1,256,512]{2,1,0:T(8,128)(2,1)} %fusion.26), channel_id=1, source_target_pairs={{0,8},{4,12},{8,16},{12,20},{16,24},{20,28},{1,9},{5,13},{9,17},{1... | collective-permute-start | bytes 786440 | tf_op jit(solution)/shard_map/ppermute | solution.py:31
  150.7 20.8 %collective-permute-start.5 = (bf16[1,256,512]{2,1,0:T(8,128)(2,1)}, bf16[1,256,512]{2,1,0:T(8,128)(2,1)S(1)}, u32[]{:S(2)}, u32[]{:S(2)}) collective-permute-start(bf16[1,256,512]{2,1,0:T(8,128)(2,1)} %fusion.24), channel_id=1, source_target_pairs={{16,0},{20,4},{24,8},{28,12},{17,1},{21,5},{25,9},{29,13},{18,2},{... | collective-permute-start | bytes 786440 | tf_op jit(solution)/shard_map/ppermute | solution.py:31
  160.4 16.1 %copy-start.8 = (f32[256,1,256]{2,0,1:T(8,128)S(1)}, f32[256,1,256]{2,0,1:T(8,128)}, u32[]{:S(2)}) copy-start(f32[256,1,256]{2,0,1:T(8,128)} %convolution_bitcast_fusion.1) | copy-start | bytes 786436
  160.4 18.0 %collective-permute-start.2 = (bf16[1,256,512]{2,1,0:T(8,128)(2,1)}, bf16[1,256,512]{2,1,0:T(8,128)(2,1)}, u32[]{:S(2)}, u32[]{:S(2)}) collective-permute-start(bf16[1,256,512]{2,1,0:T(8,128)(2,1)} %fusion.18), channel_id=1, source_target_pairs={{0,16},{4,20},{8,24},{12,28},{1,17},{5,21},{9,25},{13,29},{2,18},{... | collective-permute-start | bytes 786440 | tf_op jit(solution)/shard_map/ppermute | solution.py:31
  172.5 5.8 %copy-start.2 = (bf16[256,512]{1,0:T(8,128)(2,1)S(1)}, bf16[256,512]{1,0:T(8,128)(2,1)}, u32[]{:S(2)}) copy-start(bf16[256,512]{1,0:T(8,128)(2,1)} %copy-done.1) | copy-start | bytes 786436
  196.5 3.3 %copy-start.5 = (f32[2048,256]{1,0:T(8,128)S(1)}, f32[2048,256]{1,0:T(8,128)}, u32[]{:S(2)}) copy-start(f32[2048,256]{1,0:T(8,128)} %get-tuple-element.11) | copy-start | bytes 6291460
  199.8 2.3 %copy-start.4 = (f32[2048,256]{1,0:T(8,128)S(1)}, f32[2048,256]{1,0:T(8,128)}, u32[]{:S(2)}) copy-start(f32[2048,256]{1,0:T(8,128)} %get-tuple-element.12) | copy-start | bytes 6291460
  202.1 2.3 %copy-start.3 = (f32[256,2048]{1,0:T(8,128)S(1)}, f32[256,2048]{1,0:T(8,128)}, u32[]{:S(2)}) copy-start(f32[256,2048]{1,0:T(8,128)} %get-tuple-element.13) | copy-start | bytes 6291460
Sparse Core Ops, SparseCore 0:
  123.0 14.8 all-gather.2
  140.0 56.4 all-gather.4

commit v2 on v1

v2 whole, which is shorter than its diff:
```python
import functools
import math

import jax
import jax.numpy as jnp
from jax import lax
from jax.experimental import pallas as pl
from jax.experimental.pallas import tpu as pltpu
from jax.sharding import PartitionSpec as P

H = 4
DK = 256
DV = 512
GROUPS = 8
LINKS = 4
MESH = pl.DeviceIdType.MESH
ROWS = (((0,), (0,)), ((), ()))
COLS = (((1,), (1,)), ((), ()))


def dot(a, b, dims=(((1,), (0,)), ((), ()))):
    return lax.dot_general(a, b, dims, preferred_element_type=jnp.float32)


class Chain:
    def __init__(self, count, reverse, log_span, own, pair_in, summed, link_in, link_out, out_half,
                 state, sems):
        self.sp, self.tp = lax.axis_index("sp"), lax.axis_index("tp")
        self.y = self.sp % 2
        self.yy = self.y if reverse else 1 - self.y
        self.pairs = count // 2
        z = self.sp // 2
        self.t = self.pairs - 1 - z if reverse else z
        self.next = jnp.where(self.t < self.pairs - 1, self.sp - 2 if reverse else self.sp + 2, self.sp)
        self.decay = jnp.exp(jnp.full((8, 128), log_span, jnp.float32))[0:1, 0:1]
        self.own, self.pair_in, self.summed = own, pair_in, summed
        self.link_in, self.link_out, self.out_half, self.state = link_in, link_out, out_half, state
        self.ps, self.pr, self.ls, self.lr, self.bs, self.br = sems
        self.chunks = link_in.shape[0]
        self.wide = link_in.shape[2]

    def pair(self, src, dst, s, r):
        peer = (jnp.bitwise_xor(self.sp, 1), self.tp)
        return pltpu.make_async_remote_copy(src, dst, s, r, device_id=peer, device_id_type=MESH)

    def link(self, c):
        return pltpu.make_async_remote_copy(
            self.link_out.at[c],
            self.link_in.at[c],
            self.ls.at[c],
            self.lr.at[c],
            device_id=(self.next, self.tp),
            device_id_type=MESH,
        )

    def start(self):
        @pl.when(self.t == 0)
        def _():
            self.link_in[...] = jnp.zeros_like(self.link_in)

        self.one = self.pair(self.own.at[1 - self.y], self.pair_in, self.ps, self.pr)
        self.one.start()

    def fold(self):
        self.one.wait_recv()
        g = self.decay
        mine = jnp.where(self.yy == 0, 1.0, g) * self.own[self.y].astype(jnp.float32)
        theirs = jnp.where(self.yy == 0, g, 1.0) * self.pair_in[...].astype(jnp.float32)
        self.summed[...] = mine + theirs

    def step(self, i):
        if i >= self.pairs:
            return

        @pl.when(self.t == i)
        def _():
            for c in range(self.chunks):
                if i > 0:
                    self.link(c).wait_recv()
                if i < self.pairs - 1:
                    value = self.summed[:, c * self.wide : (c + 1) * self.wide]
                    if i > 0:
                        value = value + self.decay * self.decay * self.link_in[c].astype(jnp.float32)
                    self.link_out[c] = value.astype(jnp.bfloat16)
                    self.link(c).start()

    def finish(self):
        g = self.decay
        for c in range(self.chunks):
            cols = slice(c * self.wide, (c + 1) * self.wide)
            ahead = self.link_in[c].astype(jnp.float32)
            own = self.own[self.y, :, cols].astype(jnp.float32)
            near = self.pair_in[:, cols].astype(jnp.float32)
            mine = jnp.where(self.yy == 0, near + g * ahead, ahead)
            theirs = jnp.where(self.yy == 0, ahead, own + g * ahead)
            self.state[self.y, :, cols] = mine.astype(jnp.bfloat16)
            self.out_half[:, cols] = theirs.astype(jnp.bfloat16)
        self.two = self.pair(self.out_half, self.state.at[self.y], self.bs, self.br)
        self.two.start()

    def wait(self):
        self.pair(self.out_half, self.state.at[1 - self.y], self.bs, self.br).wait_recv()

    def drain(self):
        self.one.wait_send()
        self.two.wait_send()

        @pl.when(self.t < self.pairs - 1)
        def _():
            for c in range(self.chunks):
                self.link(c).wait_send()


def chain_scratch():
    half = DK // 2
    return [
        pltpu.VMEM((2, half, DV), jnp.bfloat16),
        pltpu.VMEM((half, DV), jnp.bfloat16),
        pltpu.VMEM((half, DV), jnp.float32),
        pltpu.VMEM((LINKS, half, DV // LINKS), jnp.bfloat16),
        pltpu.VMEM((LINKS, half, DV // LINKS), jnp.bfloat16),
        pltpu.VMEM((half, DV), jnp.bfloat16),
        pltpu.VMEM((2, half, DV), jnp.bfloat16),
        pltpu.SemaphoreType.DMA,
        pltpu.SemaphoreType.DMA,
        pltpu.SemaphoreType.DMA((LINKS,)),
        pltpu.SemaphoreType.DMA((LINKS,)),
        pltpu.SemaphoreType.DMA,
        pltpu.SemaphoreType.DMA,
    ]


def rates(tokens):
    tp = lax.axis_index("tp")
    logs, scales = [], []
    for h in range(H):
        exponent = -5.0 - h if 2 * h < H else -math.log2(tokens) - (h - H // 2)
        logs.append(math.log1p(-(2.0**exponent)))
        scales.append(math.sqrt(-math.expm1(2.0 * logs[-1])))
    log_gamma, scale = jnp.float32(logs[0]), jnp.float32(scales[0])
    for h in range(1, H):
        log_gamma = jnp.where(tp == h, jnp.float32(logs[h]), log_gamma)
        scale = jnp.where(tp == h, jnp.float32(scales[h]), scale)
    return log_gamma, scale


def positions(shape, axis):
    return lax.broadcasted_iota(jnp.int32, shape, axis).astype(jnp.float32)


def layer_kernel(
    count,
    place_ref,
    rw_ref,
    hid_ref,
    cot_ref,
    q_ref,
    k_ref,
    v_ref,
    wg_hbm,
    wu_hbm,
    wd_hbm,
    wo_hbm,
    kept_hbm,
    gg_ref,
    ug_ref,
    dg_ref,
    pg_ref,
    qg_ref,
    kg_ref,
    vg_ref,
    gg,
    ug,
    dg,
    pg,
    qg,
    kg,
    vg,
    wg,
    wu,
    wd,
    wo,
    packed,
    packed2,
    got,
    terms,
    part,
    half,
    kept,
    moving,
    other,
    ret,
    total,
    layer,
    spread,
    mixed_ref,
    flipped,
    blocks,
    near_v,
    near_k,
    load_sem,
    store_sem,
    d_s,
    d_r,
    a_s,
    a_r,
    b_s,
    b_r,
    c_s,
    c_r,
    r_s,
    r_r,
    k_s,
    k_r,
    p_s,
    p_r,
    h_s,
    h_r,
    x_s,
    x_r,
    l_s,
    l_r,
    *chain_refs,
):
    sp = lax.axis_index("sp")
    tp = lax.axis_index("tp")
    bf = jnp.bfloat16
    cap = place_ref.shape[1]
    tokens, width = hid_ref.shape
    wide = width // 4
    per = count // GROUPS
    n = per * cap
    offs = [pl.multiple_of(jnp.bitwise_xor(tp, r) * wide, wide) for r in range(4)]
    cols = [pl.ds(o, wide) for o in offs]

    places = ((wg_hbm, wg), (wu_hbm, wu), (wd_hbm, wd), (wo_hbm, wo), (kept_hbm, spread.at[0]))
    loads = [pltpu.make_async_copy(src, dst, load_sem.at[i]) for i, (src, dst) in enumerate(places)]
    for load in loads:
        load.start()

    def along_sp(m, src, dst, s, r):
        peer = (jnp.bitwise_xor(sp, m), tp)
        return pltpu.make_async_remote_copy(src, dst, s, r, device_id=peer, device_id_type=MESH)

    def along_tp(m, src, dst, s, r):
        peer = (sp, jnp.bitwise_xor(tp, m))
        return pltpu.make_async_remote_copy(src, dst, s, r, device_id=peer, device_id_type=MESH)

    barrier = pltpu.get_barrier_semaphore()
    for m in range(1, count):
        pl.semaphore_signal(
            barrier, inc=1, device_id=(jnp.bitwise_xor(sp, m), tp), device_id_type=MESH
        )
    for m in (1, 2):
        pl.semaphore_signal(
            barrier, inc=1, device_id=(sp, jnp.bitwise_xor(tp, m)), device_id_type=MESH
        )

    sends = []

    def begin(copy):
        copy.start()
        sends.append(copy)
        return copy

    def pack(m, r):
        one = place_ref[jnp.bitwise_xor(sp, m)]
        rows = dot(one, hid_ref[:, cols[r]]).astype(bf)
        ups = rw_ref[jnp.bitwise_xor(sp, m)] * dot(one, cot_ref[:, cols[r]])
        return rows, ups.astype(bf)

    packed2[0], packed2[1] = pack(1, 2)
    arrive = {}
    for m in range(1, count):
        packed[m, 0], packed[m, 1] = pack(m, 0)
        if m == 1:
            pl.semaphore_wait(barrier, count + 1)
        arrive[m] = begin(along_sp(m, packed.at[m], got.at[0, :, m], d_s.at[m], d_r.at[m]))
        if m == 1:
            arrive2 = begin(along_sp(1, packed2, got.at[2, :, 1], d_s.at[0], d_r.at[0]))
    for r in range(4):
        got[r, 0, 0], got[r, 1, 0] = pack(0, r)

    log_gamma, scale = rates(tokens * count)
    set_size = len(chain_refs) // 2
    refs = chain_refs[:set_size]
    chain = Chain(count, False, log_gamma * tokens, *refs[:7], refs[7:])
    prior_ref = refs[6]
    faded = k_ref[...] * jnp.exp(log_gamma * (tokens - positions((tokens, DK), 0)))
    refs[0][...] = dot(faded.astype(bf), v_ref[...], ROWS).astype(bf).reshape(refs[0].shape)
    chain.start()

    spreads, seen = {}, set()

    def landed(s):
        if s and s not in seen:
            seen.add(s)
            spreads[s].wait_recv()

    def pass_on(s, bits):
        landed(s)
        for bit in bits:
            to = s | bit
            spreads[to] = begin(along_sp(bit, spread.at[s], spread.at[to], k_s.at[to], k_r.at[to]))

    far = count // 2
    near_bits = [1 << i for i in range(far.bit_length() - 1)][::-1]
    loads[4].wait()
    pass_on(0, near_bits)

    from_pair, from_x, from_diag = {}, {}, {}

    def relay_first(m):
        arrive[m].wait_recv()
        if m > 1:
            from_x[m] = begin(along_tp(2, got.at[0, :, m], got.at[2, :, m], b_s.at[m], b_r.at[m]))
        from_pair[m] = begin(along_tp(1, got.at[0, :, m], got.at[1, :, m], a_s.at[m], a_r.at[m]))

    def relay_second(m):
        if m > 1:
            from_x[m].wait_recv()
        else:
            arrive2.wait_recv()
        from_diag[m] = begin(along_tp(1, got.at[2, :, m], got.at[3, :, m], c_s.at[m], c_r.at[m]))

    def slots(g):
        return range(max(1, g * per), (g + 1) * per)

    def rows_of(a, r, g):
        return got[r, a, g * per : (g + 1) * per].reshape(n, wide)

    halves, across, back = {}, {}, {}

    def expert(g):
        for m in slots(g):
            from_pair[m].wait_recv()
            from_diag[m].wait_recv()
        gate_pre = sum(dot(rows_of(0, r, g), wg[cols[r], :]) for r in range(4))
        up_pre = sum(dot(rows_of(0, r, g), wu[cols[r], :]) for r in range(4))
        unit = sum(dot(rows_of(1, r, g), wd[:, cols[r]], COLS) for r in range(4))
        sigma = jax.nn.sigmoid(gate_pre)
        active = gate_pre * sigma
        span = pl.ds(g * n, n)
        terms[0, span] = (active * up_pre).astype(bf)
        gate_term = (unit * up_pre * sigma * (1.0 + gate_pre * (1.0 - sigma))).astype(bf)
        up_term = (unit * active).astype(bf)
        terms[1, span] = gate_term
        terms[2, span] = up_term
        for at, r in ((2, 1), (3, 3), (0, 0), (1, 2)):
            piece = dot(gate_term, wg[cols[r], :], COLS) + dot(up_term, wu[cols[r], :], COLS)
            part[at, span] = piece.astype(bf)
            if at == 3:
                halves[g] = begin(
                    along_tp(1, part.at[2:4, span], half.at[:, span], h_s.at[g], h_r.at[g])
                )

    def cross(g):
        span = pl.ds(g * n, n)
        halves[g].wait_recv()
        mine = part[1, span].astype(jnp.float32) + half[1, span].astype(jnp.float32)
        moving[span] = mine.astype(bf)
        across[g] = begin(along_tp(2, moving.at[span], other.at[span], x_s.at[g], x_r.at[g]))
        mine = part[0, span].astype(jnp.float32) + half[0, span].astype(jnp.float32)
        kept[span] = mine.astype(bf)

    def give_back(g):
        across[g].wait_recv()
        for m in range(g * per, (g + 1) * per):
            span = pl.ds(m * cap, cap)
            done = (kept[span].astype(jnp.float32) + other[span].astype(jnp.float32)).astype(bf)
            if m == 0:
                ret[0] = done
            else:
                kept[span] = done
                back[m] = begin(along_sp(m, kept.at[span], ret.at[m], r_s.at[m], r_r.at[m]))

    for m in slots(0):
        relay_first(m)
        relay_second(m)
    for load in loads[:4]:
        load.wait()
    expert(0)
    middle = GROUPS // 2
    for i in range(1, GROUPS):
        for m in slots(i):
            relay_first(m)
        if i > 1:
            for m in slots(i - 1):
                relay_second(m)
        if i > 2:
            give_back(i - 3)
        if i > 1:
            cross(i - 2)
            expert(i - 1)
        if i == middle + 1:
            pass_on(0, [far])
        if i == 3:
            chain.fold()
        if 3 <= i:
            chain.step(i - 3)
    last = GROUPS - 1
    for j in range(last - 2, count // 2):
        chain.step(j)
    for s in sorted(range(2, far, 2), key=lambda s: bin(s).count("1")):
        low = s & -s
        pass_on(s, [b for b in near_bits if b < low])
    cross(last - 1)
    for m in slots(last):
        relay_second(m)
    give_back(last - 2)
    chain.finish()
    expert(last)
    give_back(last - 1)
    pass_on(far, near_bits)
    cross(last)

    def whole(a, r):
        return got[r, a].reshape(count * cap, wide)

    for r in range(4):
        dg[:, cols[r]] = dot(terms[0], whole(1, r), ROWS)
    give_back(last)
    stores = []

    def store(src, dst):
        stores.append(pltpu.make_async_copy(src, dst, store_sem.at[len(stores)]))
        stores[-1].start()

    store(dg, dg_ref)
    total[...] = cot_ref[:, cols[0]].astype(jnp.float32)
    for m in range(count):
        if m:
            back[m].wait_recv()
        total[...] += dot(place_ref[jnp.bitwise_xor(sp, m)], ret[m], ROWS)
    layer[0] = total[...].astype(bf)
    one = begin(along_tp(2, layer.at[0], layer.at[2], l_s.at[0], l_r.at[0]))
    two = begin(along_tp(1, layer.at[0], layer.at[1], l_s.at[1], l_r.at[1]))

    step = min(256, wide)
    eye = (positions((step, step), 0) == positions((step, step), 1)).astype(bf)

    def flip(r):
        for c in range(wide // step):
            at = pl.multiple_of(offs[r] + c * step, step)
            flipped[pl.ds(at, step), :] = dot(eye, layer[r, :, c * step : (c + 1) * step], COLS).astype(bf)

    total[...] = dot(layer[0], wo[cols[0], :])
    flip(0)
    two.wait_recv()
    total[...] += dot(layer[1], wo[cols[1], :])
    flip(1)
    faded = (q_ref[...] * jnp.exp(log_gamma * (positions((tokens, DK), 0) + 1.0))).astype(bf)
    for r in range(4):
        gg[cols[r], :] = dot(whole(0, r), terms[1], ROWS)
    store(gg, gg_ref)
    for s in sorted(range(far + 2, count, 2), key=lambda s: bin(s).count("1")):
        low = s & -s
        pass_on(s, [b for b in near_bits if b < low])
    one.wait_recv()
    three = begin(along_tp(1, layer.at[2], layer.at[3], l_s.at[2], l_r.at[2]))
    total[...] += dot(layer[2], wo[cols[2], :])
    flip(2)
    three.wait_recv()
    mixed_ref[...] = (total[...] + dot(layer[3], wo[cols[3], :])).astype(bf)
    refs = chain_refs[set_size:]
    ahead = Chain(count, True, log_gamma * tokens, *refs[:7], refs[7:])
    refs[0][...] = dot(faded, mixed_ref[...], ROWS).astype(bf).reshape(refs[0].shape)
    ahead.start()
    flip(3)
    rows = width // count
    share = rows // 4
    for m in range(count):
        at = pl.multiple_of(jnp.bitwise_xor(sp, m) * rows + tp * share, share)
        if m:
            arrive[m] = begin(
                along_sp(m, flipped.at[pl.ds(at, share)], blocks.at[m, 0], p_s.at[m], p_r.at[m])
            )
        else:
            blocks[0, 0] = flipped[pl.ds(at, share)]
    for r in range(4):
        ug[cols[r], :] = dot(whole(0, r), terms[2], ROWS)
    store(ug, ug_ref)
    ahead.fold()
    ahead.step(0)
    gap = positions((tokens, tokens), 0) - positions((tokens, tokens), 1)
    fade = jnp.where(gap >= 0, scale * jnp.exp(log_gamma * jnp.maximum(gap, 0.0)), 0.0)
    near_v[...] = (dot(mixed_ref[...], v_ref[...], COLS) * fade).astype(bf)
    near_k[...] = (dot(q_ref[...], k_ref[...], COLS) * fade).astype(bf)
    ahead.step(1)
    lead = scale * jnp.exp(log_gamma * positions((tokens, DK), 0))
    chain.wait()
    prior = prior_ref[...].reshape(DK, DV)
    qg[...] = dot(near_v[...], k_ref[...]) + lead * dot(mixed_ref[...], prior, COLS)
    store(qg, qg_ref)
    kg[...] = dot(near_v[...], q_ref[...], ROWS)
    vg[...] = dot(near_k[...], mixed_ref[...], ROWS)
    for m in range(1, count):
        arrive[m].wait_recv()
    over_x = begin(along_tp(2, blocks.at[:, 0], blocks.at[:, 2], l_s.at[3], l_r.at[3]))
    over_pair = begin(along_tp(1, blocks.at[:, 0], blocks.at[:, 1], l_s.at[4], l_r.at[4]))
    for i in range(2, count // 2 - 1):
        ahead.step(i)
    ahead.step(count // 2 - 1)
    ahead.finish()
    over_x.wait_recv()
    diag = begin(along_tp(1, blocks.at[:, 2], blocks.at[:, 3], l_s.at[5], l_r.at[5]))
    over_pair.wait_recv()
    diag.wait_recv()
    for s in spreads:
        landed(s)
    proj = jnp.zeros((rows, spread.shape[2]), jnp.float32)
    for m in range(count):
        proj = proj + dot(blocks[m].reshape(rows, tokens), spread[m])
    proj = proj.reshape(4, share, spread.shape[2])
    for r in range(4):
        at = pl.multiple_of(jnp.bitwise_xor(tp, r) * share, share)
        pg[pl.ds(at, share), :] = proj[r]
    store(pg, pg_ref)
    ahead.wait()
    later = refs[6][...].reshape(DK, DV)
    trail = scale * jnp.exp(log_gamma * (tokens - 1.0 - positions((tokens, DV), 0)))
    kg[...] += trail[:, :DK] * dot(v_ref[...], later, COLS)
    store(kg, kg_ref)
    vg[...] += trail * dot(k_ref[...], later)
    store(vg, vg_ref)
    for copy in sends:
        copy.wait_send()
    chain.drain()
    ahead.drain()
    for copy in stores:
        copy.wait()


def publish_kernel(count, *refs):
    srcs, dsts, tmps, sems = refs[:count], refs[count : 2 * count], refs[2 * count : -1], refs[-1]
    ins = [pltpu.make_async_copy(srcs[i], tmps[i], sems.at[0, i]) for i in range(count)]
    outs = [pltpu.make_async_copy(tmps[i], dsts[i], sems.at[1, i]) for i in range(count)]
    for copy in ins:
        copy.start()
    for i in range(count):
        ins[i].wait()
        outs[i].start()
    for copy in outs:
        copy.wait()


def publish(*arrays):
    hbm = pl.BlockSpec(memory_space=pl.ANY)
    count = len(arrays)
    return pl.pallas_call(
        functools.partial(publish_kernel, count),
        out_shape=tuple(jax.ShapeDtypeStruct(a.shape, a.dtype) for a in arrays),
        in_specs=[hbm] * count,
        out_specs=(hbm,) * count,
        scratch_shapes=[pltpu.VMEM(a.shape, a.dtype) for a in arrays]
        + [pltpu.SemaphoreType.DMA((2, count))],
        compiler_params=pltpu.CompilerParams(vmem_limit_bytes=62 * 2**20),
        name="publish",
    )(*arrays)


def whole_layer(
    place, row_weight, hidden, cotangent, queries, keys, values, gate_w, up_w, down_w, out_w, retained
):
    count = lax.axis_size("sp")
    assert lax.axis_size("tp") == 4 and count % GROUPS == 0
    cap = place.shape[1]
    tokens, width = hidden.shape
    units = gate_w.shape[1]
    wide = width // 4
    slots = count * cap
    rows, vals = width // count, retained.shape[1]
    bf, f32 = jnp.bfloat16, jnp.float32
    dma = pltpu.SemaphoreType.DMA
    vmem = pl.BlockSpec(memory_space=pltpu.VMEM)
    hbm = pl.BlockSpec(memory_space=pl.ANY)
    shape = jax.ShapeDtypeStruct
    return pl.pallas_call(
        functools.partial(layer_kernel, count),
        out_shape=(
            shape((width, units), f32),
            shape((width, units), f32),
            shape((units, width), f32),
            shape((rows, vals), f32),
            shape(queries.shape, f32),
            shape(keys.shape, f32),
            shape(values.shape, f32),
        ),
        in_specs=[vmem] * 7 + [hbm] * 5,
        out_specs=(hbm,) * 7,
        scratch_shapes=[
            pltpu.VMEM((width, units), f32),
            pltpu.VMEM((width, units), f32),
            pltpu.VMEM((units, width), f32),
            pltpu.VMEM((rows, vals), f32),
            pltpu.VMEM(queries.shape, f32),
            pltpu.VMEM(keys.shape, f32),
            pltpu.VMEM(values.shape, f32),
            pltpu.VMEM((width, units), bf),
            pltpu.VMEM((width, units), bf),
            pltpu.VMEM((units, width), bf),
            pltpu.VMEM(out_w.shape, bf),
            pltpu.VMEM((count, 2, cap, wide), bf),
            pltpu.VMEM((2, cap, wide), bf),
            pltpu.VMEM((4, 2, count, cap, wide), bf),
            pltpu.VMEM((3, slots, units), bf),
            pltpu.VMEM((4, slots, wide), bf),
            pltpu.VMEM((2, slots, wide), bf),
            pltpu.VMEM((slots, wide), bf),
            pltpu.VMEM((slots, wide), bf),
            pltpu.VMEM((slots, wide), bf),
            pltpu.VMEM((count, cap, wide), bf),
            pltpu.VMEM((tokens, wide), f32),
            pltpu.VMEM((4, tokens, wide), bf),
            pltpu.VMEM((count,) + retained.shape, bf),
            pltpu.VMEM((tokens, DV), bf),
            pltpu.VMEM((width, tokens), bf),
            pltpu.VMEM((count, 4, rows // 4, tokens), bf),
            pltpu.VMEM((tokens, tokens), bf),
            pltpu.VMEM((tokens, tokens), bf),
            dma((5,)),
            dma((7,)),
        ]
        + [dma((count,))] * 14
        + [dma((GROUPS,))] * 4
        + [dma((6,))] * 2
        + chain_scratch()
        + chain_scratch(),
        compiler_params=pltpu.CompilerParams(
            collective_id=0, has_side_effects=True, vmem_limit_bytes=62 * 2**20
        ),
        name="layer",
    )(
        place,
        row_weight,
        hidden,
        cotangent,
        queries,
        keys,
        values,
        gate_w,
        up_w,
        down_w,
        out_w,
        retained,
    )


def routing(routes, route_weight, experts_all, tok_local):
    top_count = routes.shape[1]
    capacity = 3 * tok_local * top_count // (2 * experts_all)
    capacity = -(-capacity // 16) * 16
    ids = jnp.arange(experts_all, dtype=jnp.int32)[:, None]
    named = [routes[:, r][None, :] == ids for r in range(top_count)]
    member = sum(m.astype(jnp.float32) for m in named)
    slot_weight = sum(jnp.where(m, route_weight[:, r][None, :], 0.0) for r, m in enumerate(named))
    order = jnp.arange(tok_local, dtype=jnp.int32)
    earlier = (order[:, None] < order[None, :]).astype(jnp.bfloat16)
    rank = jnp.dot(member.astype(jnp.bfloat16), earlier, preferred_element_type=jnp.float32)
    rank = jnp.where(member > 0.0, rank, -1.0).astype(jnp.int32)
    hit = rank[:, None, :] == jnp.arange(capacity, dtype=jnp.int32)[None, :, None]
    row_weight = jnp.sum(jnp.where(hit, slot_weight[:, None, :], 0.0), axis=2, keepdims=True)
    return hit.astype(jnp.bfloat16), row_weight


def local(
    hidden,
    cotangent,
    retained,
    queries,
    key_rows,
    value_rows,
    routes,
    route_weight,
    gate_weight,
    up_weight,
    down_weight,
    out_weight,
):
    experts_all = gate_weight.shape[0] * lax.axis_size("sp")
    assert gate_weight.shape[0] == 1 and queries.shape[1] == DK
    place_rows, row_weight = routing(routes, route_weight, experts_all, hidden.shape[0])
    outs = whole_layer(
        place_rows,
        row_weight,
        hidden,
        cotangent,
        queries,
        key_rows,
        value_rows,
        gate_weight[0],
        up_weight[0],
        down_weight[0],
        out_weight,
        retained,
    )
    order = (4, 5, 3, 6, 0, 1, 2)
    outs = dict(zip(order, publish(*(outs[i] for i in order))))
    gate_grad, up_grad, down_grad, proj_grad = (outs[i] for i in range(4))
    query_gradient, key_gradient, value_gradient = (outs[i] for i in range(4, 7))
    return (
        gate_grad[None],
        up_grad[None],
        down_grad[None],
        proj_grad,
        query_gradient,
        key_gradient,
        value_gradient,
    )


def solution(mesh):
    return jax.shard_map(
        local,
        mesh=mesh,
        in_specs=(
            P("sp", None),
            P("sp", None),
            P("sp", "tp"),
            P("sp", "tp"),
            P("sp", "tp"),
            P("sp", "tp"),
            P("sp", None),
            P("sp", None),
            P("sp", None, "tp"),
            P("sp", None, "tp"),
            P("sp", "tp", None),
            P(None, "tp"),
        ),
        out_specs=(
            P("sp", None, "tp"),
            P("sp", None, "tp"),
            P("sp", "tp", None),
            P("sp", "tp"),
            P("sp", "tp"),
            P("sp", "tp"),
            P("sp", "tp"),
        ),
        check_vma=False,
    )
```

time: 213 us -> 122 us (0.57)
  waiting for transfers between devices: 26.6 us -> 0 us
  Pallas kernels: 93.6 us -> 117 us
  starting transfers between devices: 20.5 us -> 0 us
  matrix products: 18.1 us -> 0.15 us
  blocking collectives: 16.3 us -> 0 us
  between operations: 14.6 us -> 0.81 us
  local copies, waits for them, and re-layouts: 13.2 us -> 2.47 us
  other arithmetic: 9.8 us -> 1.07 us
    pallas_call x1 -> x2, Pallas kernels: 93.6 us -> 117 us  [the longest x1 111 us: whole_layer(): pl.pallas_call(functools.partial(layer_kernel, count), out_shape=(shape((...]
    ppermute x6 -> x0, starting transfers between devices: 20.2 us -> none  [carried(): lax.ppermute(held.astype(jnp.bfloat16), axis, pairs).astype(jnp.float32)]
    dot_general x11 -> x0, matrix products: 17.9 us -> none  [the longest x1 3.26 us: local(): lax.dot_general(block_all.reshape(sp_count * tok_local, -1), retained_all...]
    all_to_all x1 -> x0, blocking collectives: 16.3 us -> none  [local(): lax.all_to_all(share_rows, 'sp', split_axis=0, concat_axis=0, tiled=True)]
    all_gather x2 -> x0, waiting for transfers between devices: 14.4 us -> none  [the longest x1 14.4 us: local(): retained_all = lax.all_gather(retained, 'sp', axis=0, tiled=True)]
    ppermute x6 -> x0, waiting for transfers between devices: 11.6 us -> none  [carried(): lax.ppermute(held.astype(jnp.bfloat16), axis, pairs).astype(jnp.float32)]
    convert_element_type x6 -> x0, other arithmetic: 7.6 us -> none  [carried(): held.astype(jnp.bfloat16)]
    unnamed x23 -> x0, local copies, waits for them, and re-layouts: 7.34 us -> none
  transfers between devices with their start and end apart: 8 -> 0, of which waited for: 3 -> 0; matrix products, arithmetic and copies ran while one was open for 12% -> 0% of each run, Pallas kernels for 0% -> 0%
where the time goes in v2:
time: 122 us
  Pallas kernels  117 us (96%)
  local copies, waits for them, and re-layouts  2.47 us (2%)
    pallas_call x1, Pallas kernels, whole_layer(): pl.pallas_call(functools.partial(layer_kernel, count), out_shape=(shape((...  111 us
    pallas_call x1, Pallas kernels, publish(): pl.pallas_call(functools.partial(publish_kernel, count), out_shape=tuple(...  6.46 us

profile of v2, /device:TPU:0, one launch (start us, length us, event | category | flops | bytes accessed | tf_op | source)
XLA Modules:
  0.0 121.7 jit_solution(16745318738459735519)
XLA Ops:
  0.6 0.8 fusion.8
  1.4 0.8 fusion.7
  2.2 0.2 fusion
  2.3 0.2 select_reduce_fusion
  2.5 0.8 fusion.1.place_ref
  3.4 0.9 copy.19.rw_ref
  4.3 110.8 %layer.1 = (f32[2048,256]{1,0:T(8,128)}, f32[2048,256]{1,0:T(8,128)}, f32[256,2048]{1,0:T(8,128)}, f32[256,512]{1,0:T(8,128)}, f32[256,256]{1,0:T(8,128)}, /*index=5*/f32[256,256]{1,0:T(8,128)}, f32[256,512]{1,0:T(8,128)}) custom-call(bf16[8,96,256]{2,1,0:T(8,128)(2,1)} %fusion.1.place_ref, f32[8,96,1]{2,1,0:T(8,128)} %copy.19.rw_ref, ...), custom_call_target="tpu_custom_call" | custom-call | tf_op jit(solution)/shard_map/layer/pallas_call | solution.py:578
  115.1 6.5 %publish.1 = (f32[256,256]{1,0:T(8,128)}, f32[256,256]{1,0:T(8,128)}, f32[256,512]{1,0:T(8,128)}, f32[256,512]{1,0:T(8,128)}, f32[2048,256]{1,0:T(8,128)}, /*index=5*/f32[2048,256]{1,0:T(8,128)}, f32[256,2048]{1,0:T(8,128)}) custom-call(f32[256,256]{1,0:T(8,128)} %get-tuple-element.21.refs_0_, f32[256,256]{1,0:T(8,128)} %get-tuple-element.22.refs_1_, ...), custom_call_target="tpu_custom_call" | custom-call | tf_op jit(solution)/shard_map/publish/pallas_call | solution.py:550
  (1 shorter events, 0.0 us)

commit v3 on v2

--- a/solution.py
+++ b/solution.py
@@ -150,25 +150,19 @@
 
 def layer_kernel(
     count,
-    place_ref,
-    rw_ref,
-    hid_ref,
-    cot_ref,
-    q_ref,
-    k_ref,
-    v_ref,
+    cap,
+    routes_ref,
+    weight_ref,
+    hid_hbm,
+    cot_hbm,
+    q_hbm,
+    k_hbm,
+    v_hbm,
     wg_hbm,
     wu_hbm,
     wd_hbm,
     wo_hbm,
     kept_hbm,
-    gg_ref,
-    ug_ref,
-    dg_ref,
-    pg_ref,
-    qg_ref,
-    kg_ref,
-    vg_ref,
     gg,
     ug,
     dg,
@@ -176,6 +170,12 @@
     qg,
     kg,
     vg,
+    place_ref,
+    hid_ref,
+    cot_ref,
+    q_ref,
+    k_ref,
+    v_ref,
     wg,
     wu,
     wd,
@@ -199,7 +199,6 @@
     near_v,
     near_k,
     load_sem,
-    store_sem,
     d_s,
     d_r,
     a_s,
@@ -225,15 +224,25 @@
     sp = lax.axis_index("sp")
     tp = lax.axis_index("tp")
     bf = jnp.bfloat16
-    cap = place_ref.shape[1]
-    tokens, width = hid_ref.shape
+    tokens, width = hid_hbm.shape
     wide = width // 4
     per = count // GROUPS
     n = per * cap
     offs = [pl.multiple_of(jnp.bitwise_xor(tp, r) * wide, wide) for r in range(4)]
     cols = [pl.ds(o, wide) for o in offs]
 
-    places = ((wg_hbm, wg), (wu_hbm, wu), (wd_hbm, wd), (wo_hbm, wo), (kept_hbm, spread.at[0]))
+    places = (
+        (hid_hbm, hid_ref),
+        (cot_hbm, cot_ref),
+        (k_hbm, k_ref),
+        (v_hbm, v_ref),
+        (wg_hbm, wg),
+        (wu_hbm, wu),
+        (wd_hbm, wd),
+        (kept_hbm, spread.at[0]),
+        (q_hbm, q_ref),
+        (wo_hbm, wo),
+    )
     loads = [pltpu.make_async_copy(src, dst, load_sem.at[i]) for i, (src, dst) in enumerate(places)]
     for load in loads:
         load.start()
@@ -263,17 +272,36 @@
         sends.append(copy)
         return copy
 
+    top = routes_ref.shape[0]
+    ids = lax.broadcasted_iota(jnp.int32, (count, tokens), 0)
+    named = [jnp.bitwise_xor(routes_ref[r : r + 1, :], sp) == ids for r in range(top)]
+    member = sum(jnp.where(hit, 1.0, 0.0) for hit in named)
+    slot_weight = sum(
+        jnp.where(hit, weight_ref[r : r + 1, :], 0.0) for r, hit in enumerate(named)
+    )
+    earlier = positions((tokens, tokens), 0) < positions((tokens, tokens), 1)
+    rank = dot(member.astype(bf), jnp.where(earlier, 1.0, 0.0).astype(bf))
+    rank = jnp.where(member > 0.0, rank, -1.0)
+    rows_at = positions((cap, tokens), 0)
+    scales = {}
+    for m in range(count):
+        hit = rank[m : m + 1, :] == rows_at
+        place_ref[m] = jnp.where(hit, 1.0, 0.0).astype(bf)
+        scales[m] = jnp.sum(jnp.where(hit, slot_weight[m : m + 1, :], 0.0), axis=1, keepdims=True)
+
     def pack(m, r):
-        one = place_ref[jnp.bitwise_xor(sp, m)]
+        one = place_ref[m]
         rows = dot(one, hid_ref[:, cols[r]]).astype(bf)
-        ups = rw_ref[jnp.bitwise_xor(sp, m)] * dot(one, cot_ref[:, cols[r]])
-        return rows, ups.astype(bf)
-
-    packed2[0], packed2[1] = pack(1, 2)
+        return rows, (scales[m] * dot(one, cot_ref[:, cols[r]])).astype(bf)
+
+    loads[0].wait()
+    loads[1].wait()
     arrive = {}
-    for m in range(1, count):
+    for m in list(range(2, count)) + [1]:
         packed[m, 0], packed[m, 1] = pack(m, 0)
         if m == 1:
+            packed2[0], packed2[1] = pack(1, 2)
+        if m == 2:
             pl.semaphore_wait(barrier, count + 1)
         arrive[m] = begin(along_sp(m, packed.at[m], got.at[0, :, m], d_s.at[m], d_r.at[m]))
         if m == 1:
@@ -286,6 +314,8 @@
     refs = chain_refs[:set_size]
     chain = Chain(count, False, log_gamma * tokens, *refs[:7], refs[7:])
     prior_ref = refs[6]
+    for load in loads[2:4]:
+        load.wait()
     faded = k_ref[...] * jnp.exp(log_gamma * (tokens - positions((tokens, DK), 0)))
     refs[0][...] = dot(faded.astype(bf), v_ref[...], ROWS).astype(bf).reshape(refs[0].shape)
     chain.start()
@@ -305,7 +335,7 @@
 
     far = count // 2
     near_bits = [1 << i for i in range(far.bit_length() - 1)][::-1]
-    loads[4].wait()
+    loads[7].wait()
     pass_on(0, near_bits)
 
     from_pair, from_x, from_diag = {}, {}, {}
@@ -377,64 +407,63 @@
     for m in slots(0):
         relay_first(m)
         relay_second(m)
-    for load in loads[:4]:
+    for load in loads[4:7] + loads[8:]:
         load.wait()
     expert(0)
-    middle = GROUPS // 2
-    for i in range(1, GROUPS):
-        for m in slots(i):
+    turns = [0] + list(range(2, GROUPS))
+    for i in range(1, GROUPS - 1):
+        for m in slots(turns[i]):
             relay_first(m)
         if i > 1:
-            for m in slots(i - 1):
+            for m in slots(turns[i - 1]):
                 relay_second(m)
         if i > 2:
-            give_back(i - 3)
+            give_back(turns[i - 3])
+        if i == 1:
+            cross(0)
+        elif i > 2:
+            cross(turns[i - 2])
         if i > 1:
-            cross(i - 2)
-            expert(i - 1)
-        if i == middle + 1:
+            expert(turns[i - 1])
+        if i == GROUPS // 2:
             pass_on(0, [far])
-        if i == 3:
-            chain.fold()
-        if 3 <= i:
-            chain.step(i - 3)
-    last = GROUPS - 1
-    for j in range(last - 2, count // 2):
-        chain.step(j)
     for s in sorted(range(2, far, 2), key=lambda s: bin(s).count("1")):
         low = s & -s
         pass_on(s, [b for b in near_bits if b < low])
-    cross(last - 1)
-    for m in slots(last):
+    for m in slots(1):
+        relay_first(m)
         relay_second(m)
-    give_back(last - 2)
-    chain.finish()
-    expert(last)
-    give_back(last - 1)
+    give_back(turns[-3])
+    cross(turns[-2])
+    expert(1)
+    chain.fold()
+    chain.step(0)
+    for m in slots(turns[-1]):
+        relay_second(m)
+    cross(1)
+    give_back(turns[-2])
+    expert(turns[-1])
+    give_back(1)
     pass_on(far, near_bits)
-    cross(last)
+    cross(turns[-1])
 
     def whole(a, r):
         return got[r, a].reshape(count * cap, wide)
 
     for r in range(4):
         dg[:, cols[r]] = dot(terms[0], whole(1, r), ROWS)
-    give_back(last)
-    stores = []
-
-    def store(src, dst):
-        stores.append(pltpu.make_async_copy(src, dst, store_sem.at[len(stores)]))
-        stores[-1].start()
-
-    store(dg, dg_ref)
+    give_back(turns[-1])
+    chain.step(1)
     total[...] = cot_ref[:, cols[0]].astype(jnp.float32)
     for m in range(count):
         if m:
             back[m].wait_recv()
-        total[...] += dot(place_ref[jnp.bitwise_xor(sp, m)], ret[m], ROWS)
+        total[...] += dot(place_ref[m], ret[m], ROWS)
     layer[0] = total[...].astype(bf)
     one = begin(along_tp(2, layer.at[0], layer.at[2], l_s.at[0], l_r.at[0]))
     two = begin(along_tp(1, layer.at[0], layer.at[1], l_s.at[1], l_r.at[1]))
+    for j in range(2, count // 2 - 1):
+        chain.step(j)
 
     step = min(256, wide)
     eye = (positions((step, step), 0) == positions((step, step), 1)).astype(bf)
@@ -452,10 +481,11 @@
     faded = (q_ref[...] * jnp.exp(log_gamma * (positions((tokens, DK), 0) + 1.0))).astype(bf)
     for r in range(4):
         gg[cols[r], :] = dot(whole(0, r), terms[1], ROWS)
-    store(gg, gg_ref)
     for s in sorted(range(far + 2, count, 2), key=lambda s: bin(s).count("1")):
         low = s & -s
         pass_on(s, [b for b in near_bits if b < low])
+    chain.step(count // 2 - 1)
+    chain.finish()
     one.wait_recv()
     three = begin(along_tp(1, layer.at[2], layer.at[3], l_s.at[2], l_r.at[2]))
     total[...] += dot(layer[2], wo[cols[2], :])
@@ -479,7 +509,6 @@
             blocks[0, 0] = flipped[pl.ds(at, share)]
     for r in range(4):
         ug[cols[r], :] = dot(whole(0, r), terms[2], ROWS)
-    store(ug, ug_ref)
     ahead.fold()
     ahead.step(0)
     gap = positions((tokens, tokens), 0) - positions((tokens, tokens), 1)
@@ -491,7 +520,6 @@
     chain.wait()
     prior = prior_ref[...].reshape(DK, DV)
     qg[...] = dot(near_v[...], k_ref[...]) + lead * dot(mixed_ref[...], prior, COLS)
-    store(qg, qg_ref)
     kg[...] = dot(near_v[...], q_ref[...], ROWS)
     vg[...] = dot(near_k[...], mixed_ref[...], ROWS)
     for m in range(1, count):
@@ -515,57 +543,47 @@
     for r in range(4):
         at = pl.multiple_of(jnp.bitwise_xor(tp, r) * share, share)
         pg[pl.ds(at, share), :] = proj[r]
-    store(pg, pg_ref)
     ahead.wait()
     later = refs[6][...].reshape(DK, DV)
     trail = scale * jnp.exp(log_gamma * (tokens - 1.0 - positions((tokens, DV), 0)))
     kg[...] += trail[:, :DK] * dot(v_ref[...], later, COLS)
-    store(kg, kg_ref)
     vg[...] += trail * dot(k_ref[...], later)
-    store(vg, vg_ref)
     for copy in sends:
         copy.wait_send()
     chain.drain()
     ahead.drain()
-    for copy in stores:
-        copy.wait()
 
 
 def publish_kernel(count, *refs):
-    srcs, dsts, tmps, sems = refs[:count], refs[count : 2 * count], refs[2 * count : -1], refs[-1]
-    ins = [pltpu.make_async_copy(srcs[i], tmps[i], sems.at[0, i]) for i in range(count)]
-    outs = [pltpu.make_async_copy(tmps[i], dsts[i], sems.at[1, i]) for i in range(count)]
-    for copy in ins:
+    srcs, dsts, sems = refs[:count], refs[count : 2 * count], refs[-1]
+    outs = [pltpu.make_async_copy(srcs[i], dsts[i], sems.at[i]) for i in range(count)]
+    for copy in outs:
         copy.start()
-    for i in range(count):
-        ins[i].wait()
-        outs[i].start()
     for copy in outs:
         copy.wait()
 
 
 def publish(*arrays):
-    hbm = pl.BlockSpec(memory_space=pl.ANY)
     count = len(arrays)
     return pl.pallas_call(
         functools.partial(publish_kernel, count),
         out_shape=tuple(jax.ShapeDtypeStruct(a.shape, a.dtype) for a in arrays),
-        in_specs=[hbm] * count,
-        out_specs=(hbm,) * count,
-        scratch_shapes=[pltpu.VMEM(a.shape, a.dtype) for a in arrays]
-        + [pltpu.SemaphoreType.DMA((2, count))],
-        compiler_params=pltpu.CompilerParams(vmem_limit_bytes=62 * 2**20),
+        in_specs=[pl.BlockSpec(memory_space=pltpu.VMEM)] * count,
+        out_specs=(pl.BlockSpec(memory_space=pl.ANY),) * count,
+        scratch_shapes=[pltpu.SemaphoreType.DMA((count,))],
+        compiler_params=pltpu.CompilerParams(vmem_limit_bytes=16 * 2**20),
         name="publish",
     )(*arrays)
 
 
 def whole_layer(
-    place, row_weight, hidden, cotangent, queries, keys, values, gate_w, up_w, down_w, out_w, retained
+    routes, route_weight, hidden, cotangent, queries, keys, values, gate_w, up_w, down_w, out_w, retained
 ):
     count = lax.axis_size("sp")
     assert lax.axis_size("tp") == 4 and count % GROUPS == 0
-    cap = place.shape[1]
     tokens, width = hidden.shape
+    cap = 3 * tokens * routes.shape[1] // (2 * count)
+    cap = -(-cap // 16) * 16
     units = gate_w.shape[1]
     wide = width // 4
     slots = count * cap
@@ -574,9 +592,9 @@
     dma = pltpu.SemaphoreType.DMA
     vmem = pl.BlockSpec(memory_space=pltpu.VMEM)
     hbm = pl.BlockSpec(memory_space=pl.ANY)
-    shape = jax.ShapeDtypeStruct
+    shape = pltpu.VMEM
     return pl.pallas_call(
-        functools.partial(layer_kernel, count),
+        functools.partial(layer_kernel, count, cap),
         out_shape=(
             shape((width, units), f32),
             shape((width, units), f32),
@@ -586,16 +604,15 @@
             shape(keys.shape, f32),
             shape(values.shape, f32),
         ),
-        in_specs=[vmem] * 7 + [hbm] * 5,
-        out_specs=(hbm,) * 7,
+        in_specs=[vmem] * 2 + [hbm] * 10,
+        out_specs=(vmem,) * 7,
         scratch_shapes=[
-            pltpu.VMEM((width, units), f32),
-            pltpu.VMEM((width, units), f32),
-            pltpu.VMEM((units, width), f32),
-            pltpu.VMEM((rows, vals), f32),
-            pltpu.VMEM(queries.shape, f32),
-            pltpu.VMEM(keys.shape, f32),
-            pltpu.VMEM(values.shape, f32),
+            pltpu.VMEM((count, cap, tokens), bf),
+            pltpu.VMEM((tokens, width), bf),
+            pltpu.VMEM((tokens, width), bf),
+            pltpu.VMEM(queries.shape, bf),
+            pltpu.VMEM(keys.shape, bf),
+            pltpu.VMEM(values.shape, bf),
             pltpu.VMEM((width, units), bf),
             pltpu.VMEM((width, units), bf),
             pltpu.VMEM((units, width), bf),
@@ -618,8 +635,7 @@
             pltpu.VMEM((count, 4, rows // 4, tokens), bf),
             pltpu.VMEM((tokens, tokens), bf),
             pltpu.VMEM((tokens, tokens), bf),
-            dma((5,)),
-            dma((7,)),
+            dma((10,)),
         ]
         + [dma((count,))] * 14
         + [dma((GROUPS,))] * 4
@@ -627,12 +643,12 @@
         + chain_scratch()
         + chain_scratch(),
         compiler_params=pltpu.CompilerParams(
-            collective_id=0, has_side_effects=True, vmem_limit_bytes=62 * 2**20
+            collective_id=0, has_side_effects=True, vmem_limit_bytes=52 * 2**20
         ),
         name="layer",
     )(
-        place,
-        row_weight,
+        routes.T,
+        route_weight.T,
         hidden,
         cotangent,
         queries,
@@ -644,23 +660,6 @@
         out_w,
         retained,
     )
-
-
-def routing(routes, route_weight, experts_all, tok_local):
-    top_count = routes.shape[1]
-    capacity = 3 * tok_local * top_count // (2 * experts_all)
-    capacity = -(-capacity // 16) * 16
-    ids = jnp.arange(experts_all, dtype=jnp.int32)[:, None]
-    named = [routes[:, r][None, :] == ids for r in range(top_count)]
-    member = sum(m.astype(jnp.float32) for m in named)
-    slot_weight = sum(jnp.where(m, route_weight[:, r][None, :], 0.0) for r, m in enumerate(named))
-    order = jnp.arange(tok_local, dtype=jnp.int32)
-    earlier = (order[:, None] < order[None, :]).astype(jnp.bfloat16)
-    rank = jnp.dot(member.astype(jnp.bfloat16), earlier, preferred_element_type=jnp.float32)
-    rank = jnp.where(member > 0.0, rank, -1.0).astype(jnp.int32)
-    hit = rank[:, None, :] == jnp.arange(capacity, dtype=jnp.int32)[None, :, None]
-    row_weight = jnp.sum(jnp.where(hit, slot_weight[:, None, :], 0.0), axis=2, keepdims=True)
-    return hit.astype(jnp.bfloat16), row_weight
 
 
 def local(
@@ -677,12 +676,10 @@
     down_weight,
     out_weight,
 ):
-    experts_all = gate_weight.shape[0] * lax.axis_size("sp")
     assert gate_weight.shape[0] == 1 and queries.shape[1] == DK
-    place_rows, row_weight = routing(routes, route_weight, experts_all, hidden.shape[0])
     outs = whole_layer(
-        place_rows,
-        row_weight,
+        routes,
+        route_weight,
         hidden,
         cotangent,
         queries,

time: 122 us -> 115 us (0.943)
  Pallas kernels: 117 us -> 114 us
  local copies, waits for them, and re-layouts: 2.47 us -> 0 us
    pallas_call x1, Pallas kernels: 6.46 us -> 3.28 us  [publish(): pl.pallas_call(functools.partial(publish_kernel, count), out_shape=tuple(...]
    slice x2 -> x0, local copies, waits for them, and re-layouts: 1.52 us -> none  [the longest x1 0.76 us: routing(): named = [routes[:, r][None, :] == ids for r in range(top_count)]]
where the time goes in v3:
time: 115 us; the launch traced here: 114 us
  Pallas kernels  114 us (99%)
    pallas_call x1, Pallas kernels, whole_layer(): pl.pallas_call(functools.partial(layer_kernel, count, cap), out_shape=(sh...  110 us
    pallas_call x1, Pallas kernels, publish(): pl.pallas_call(functools.partial(publish_kernel, count), out_shape=tuple(...  3.28 us

profile of v3, /device:TPU:0, one launch (start us, length us, event | category | flops | bytes accessed | tf_op | source)
XLA Modules:
  0.0 114.5 jit_solution(12282397011153414394)
XLA Ops:
  0.6 110.4 %layer.1 = (f32[2048,256]{1,0:T(8,128)S(1)}, f32[2048,256]{1,0:T(8,128)S(1)}, f32[256,2048]{1,0:T(8,128)S(1)}, f32[256,512]{1,0:T(8,128)S(1)}, f32[256,256]{1,0:...) custom-call(s32[2,256]{1,0:T(2,128)} %bitcast.11, f32[2,256]{1,0:T(2,128)} %bitcast.12, ...), custom_call_target="tpu_custom_call" | custom-call | tf_op jit(solution)/shard_map/layer/pallas_call | solution.py:596
  111.0 3.3 %publish.1 = (f32[256,256]{1,0:T(8,128)}, f32[256,256]{1,0:T(8,128)}, f32[256,512]{1,0:T(8,128)}, f32[256,512]{1,0:T(8,128)}, f32[2048,256]{1,0:T(8,128)}, /*index=5*/f32[2048,256]{1,0:T(8,128)}, f32[256,2048]{1,0:T(8,128)}) custom-call(f32[256,256]{1,0:T(8,128)S(1)} %get-tuple-element.21.refs_0_, f32[256,256]{1,0:T(8,128)S(1)} %get-tuple-element.22.refs_1_, ...), custom_call_target="tpu_custom_call" | custom-call | tf_op jit(solution)/shard_map/publish/pallas_call | solution.py:568
